TPU v7x, 512 devices: a whole 4x8x8 slice. The times are simulated.
512 devices in a mesh: gr: 2 (over z_hi), fs: 32 (over z_lo, y), tp: 8 (over x, core).
Axes of the slice: x: 4, y: 8, z: 8 (z_hi: 2, z_lo: 4; z = z_hi * 4 + z_lo), core: 2. Of those that a mesh axis runs over, the one named last changes fastest.
Arguments:
- prompt: bfloat16 [16, 256, 2048], P(('gr', 'tp')), as said below
- norm_gain: float32 [2, 2048], P(None, 'fs'), may hold values from 0.1 to 1.9
- gate_weight: float32 [2, 2048, 4096], P(None, 'fs', ('gr', 'tp')), may hold values from -0.125 to 0.125
- up_weight: float32 [2, 2048, 4096], P(None, 'fs', ('gr', 'tp')), may hold values from -0.125 to 0.125
- down_weight: float32 [2, 4096, 2048], P(None, 'fs', ('gr', 'tp')), may hold values from -0.09375 to 0.09375
Outputs:
- gate_sampler: bfloat16 [2, 2048, 4096], P(None, None, 'fs')
- up_sampler: bfloat16 [2, 2048, 4096], P(None, None, 'fs')
- down_sampler: bfloat16 [2, 4096, 2048], P(None, 'fs')
- mixed: bfloat16 [16, 256, 2048], P(('gr', 'tp'))
Inputs may be any that keep to these rules, and one draw needn't show every extreme that they name: prompt features have scales that differ from feature to feature.
All inputs are finite; a program needn't handle non-finite values.
Results may differ from a plain program's by a relative error of at most 0.0043.
Values may be sent and summed in bfloat16 or wider, within the bound.
No kernel may reach another device: no remote copies, remote signals or barrier semaphores. Data moves between devices by JAX's collectives and lax.ppermute only.
A program may use at most 64 MiB of HBM per device.

v0:
```python
import jax
import jax.numpy as jnp
from jax import lax
from jax.sharding import PartitionSpec as P

norm_eps = 1e-06


def side_by_side(arrays, axis, dim, along):
    both = jnp.concatenate(arrays, axis=along)
    whole, at, finished = (lax.all_gather(both, axis, axis=dim, tiled=True), 0, [])
    for a in arrays:
        finished.append(lax.slice_in_dim(whole, at, at + a.shape[along], axis=along))
        at += a.shape[along]
    return tuple(finished)


def in_blocks(value, dim, count):
    shape = value.shape
    tiles = value.reshape(*shape[:dim], count, shape[dim] // count, *shape[dim + 1 :])
    return jnp.moveaxis(tiles, dim, 0)


def sum_at_owner(value, axis, dim):
    count = lax.axis_size(axis)
    tiles = lax.all_to_all(in_blocks(value, dim, count), axis, 0, 0, tiled=True)
    return jnp.sum(tiles.astype(jnp.float32), axis=0)


def from_everyone(value, axis):
    count = lax.axis_size(axis)
    return lax.all_to_all(
        jnp.broadcast_to(value[None], (count, *value.shape)), axis, 0, 0, tiled=True
    )


def taken_together(value, axis):
    everything = from_everyone(value, axis)
    return jnp.sum(everything, axis=0)


def laid_out(tiles, dim):
    shape = list(tiles.shape[1:])
    shape[dim] *= tiles.shape[0]
    return jnp.moveaxis(tiles, 0, dim).reshape(shape)


def gather_directly(value, axis, dim):
    return laid_out(from_everyone(value, axis), dim)


def per_device(prompt, norm_gain, gate_weight, up_weight, down_weight):
    width = prompt.shape[2]
    stream = prompt.reshape(-1, width).astype(jnp.float32)
    normed = (
        stream * lax.rsqrt(jnp.mean(stream * stream, axis=-1, keepdims=True) + norm_eps)
    ).astype(jnp.bfloat16)
    col_count = width // lax.axis_size("fs")
    col_start = lax.axis_index("fs") * col_count
    columns = lax.dynamic_slice_in_dim(stream, col_start, col_count, 1)
    mixed = prompt
    gate_list = []
    up_list = []
    down_list = []
    for half_step in range(2):
        gain_col = norm_gain[half_step][:, None]
        gate_bf = (gain_col * gate_weight[half_step]).astype(jnp.bfloat16)
        up_bf = (gain_col * up_weight[half_step]).astype(jnp.bfloat16)
        down_bf = down_weight[half_step].astype(jnp.bfloat16)
        gate_all, up_all, down_new = (
            *side_by_side((gate_bf, up_bf), ("gr", "tp"), 1, 0),
            lax.all_gather(down_bf, ("gr", "tp"), axis=1, tiled=True),
        )
        gate_new, up_new = (
            lax.all_to_all(gate_all, "fs", split_axis=1, concat_axis=0, tiled=True),
            lax.all_to_all(up_all, "fs", split_axis=1, concat_axis=0, tiled=True),
        )
        gate_list.append(gate_new)
        up_list.append(up_new)
        down_list.append(down_new)
        gate_act = jnp.dot(normed, gate_new, preferred_element_type=jnp.float32)
        up_act = jnp.dot(normed, up_new, preferred_element_type=jnp.float32)
        hidden = (jax.nn.silu(gate_act) * up_act).astype(jnp.bfloat16)
        partial_value = jnp.dot(hidden, down_new, preferred_element_type=jnp.float32)
        summed = sum_at_owner(partial_value.astype(jnp.bfloat16), "fs", 1)
        columns = columns + 0.5 * summed
        if half_step == 0:
            squares = taken_together(jnp.sum(columns * columns, axis=1, keepdims=True), "fs")
            normed_part = (columns * lax.rsqrt(squares / width + norm_eps)).astype(jnp.bfloat16)
            normed = gather_directly(normed_part, "fs", 1)
        else:
            mixed = gather_directly(columns.astype(jnp.bfloat16), "fs", 1).reshape(prompt.shape)
    return (jnp.stack(gate_list), jnp.stack(up_list), jnp.stack(down_list), mixed)


def solution(mesh):
    in_specs = (
        P(("gr", "tp"), None, None),
        P(None, "fs"),
        P(None, "fs", ("gr", "tp")),
        P(None, "fs", ("gr", "tp")),
        P(None, "fs", ("gr", "tp")),
    )
    out_specs = (
        P(None, None, "fs"),
        P(None, None, "fs"),
        P(None, "fs", None),
        P(("gr", "tp"), None, None),
    )
    return jax.shard_map(
        per_device, mesh=mesh, in_specs=in_specs, out_specs=out_specs, check_vma=False
    )
```

profile of v0, /device:TPU:8, one launch (start us, length us, event | category | flops | bytes accessed | tf_op | source)
XLA Modules:
  0.0 410.3 jit_solution(2993411757497262500)
XLA Ops:
  9.7 68.5 %all-gather.5.cloned.1.call-done = bf16[128,4096]{1,0:T(8,128)(2,1)} async-done(((bf16[128,256]{1,0:T(8,128)(2,1)}), bf16[128,4096]{1,0:T(8,128)(2,1)}) %all-gather.5.cloned.1.call-update) | async-done | bytes 1048592 | tf_op jit(solution)/shard_map/all_gather | solution.py:11
  78.1 1.3 slice_bitcast_fusion.1
  80.3 7.9 %all-to-all-start = ((bf16[64,32,128]{2,0,1:T(8,128)(2,1)}), bf16[64,32,128]{2,0,1:T(8,128)(2,1)S(1)}, u32[]{:S(2)}, u32[]{:S(2)}) async-start(bf16[64,32,128]{2,0,1:T(8,128)(2,1)} %bitcast.101), calls=%async_computation | async-start | bytes 1048576 | tf_op jit(solution)/shard_map/all_to_all | solution.py:75
  88.2 1.5 copy.32
  90.7 15.5 %all-to-all-done = bf16[64,32,128]{2,0,1:T(8,128)(2,1)S(1)} async-done(((bf16[64,32,128]{2,0,1:T(8,128)(2,1)}), bf16[64,32,128]{2,0,1:T(8,128)(2,1)S(1)}, u32[]{:S(2)}, u32[]{:S(2)}) %all-to-all-start) | async-done | bytes 524320 | tf_op jit(solution)/shard_map/all_to_all | solution.py:75
  106.1 4.7 %all-to-all-start.2 = ((bf16[64,32,128]{2,0,1:T(8,128)(2,1)}), bf16[64,32,128]{2,0,1:T(8,128)(2,1)S(1)}, u32[]{:S(2)}, u32[]{:S(2)}) async-start(bf16[64,32,128]{2,0,1:T(8,128)(2,1)} %bitcast.99), calls=%async_computation.2 | async-start | bytes 1048576 | tf_op jit(solution)/shard_map/all_to_all | solution.py:76
  111.2 30.8 %all-gather = bf16[1,128,2048]{2,1,0:T(8,128)(2,1)S(1)} all-gather(bf16[1,128,128]{2,1,0:T(8,128)(2,1)S(1)} %get-tuple-element.26), channel_id=2, replica_groups=mesh['gr'=2,'fs'=32,'tp'=8] {'gr','tp'}, dimensions={2}, use_global_device_ids=true | all-gather | bytes 557056 | tf_op jit(solution)/shard_map/all_gather | solution.py:72
  143.4 1.3 copy.33
  144.7 13.4 %all-to-all-start.4 = ((bf16[32,256,64]{1,2,0:T(8,128)(2,1)}), bf16[32,256,64]{1,2,0:T(8,128)(2,1)S(1)}, u32[]{:S(2)}, u32[]{:S(2)}) async-start(bf16[32,256,64]{1,2,0:T(8,128)(2,1)} %bitcast.105), calls=%async_computation.4 | async-start | bytes 2097152 | tf_op jit(solution)/shard_map/all_to_all | solution.py:26
  158.8 1.5 convert_element_type.63
  160.3 26.9 %all-to-all-done.4 = bf16[32,256,64]{1,2,0:T(8,128)(2,1)S(1)} async-done(((bf16[32,256,64]{1,2,0:T(8,128)(2,1)}), bf16[32,256,64]{1,2,0:T(8,128)(2,1)S(1)}, u32[]{:S(2)}, u32[]{:S(2)}) %all-to-all-start.4) | async-done | bytes 1048608 | tf_op jit(solution)/shard_map/all_to_all | solution.py:26
  188.9 6.1 %all-to-all-start.5 = ((f32[32,256,1]{1,2,0:T(1,128)}), f32[32,256,1]{1,2,0:T(1,128)S(1)}, u32[]{:S(2)}, u32[]{:S(2)}) async-start(f32[32,256,1]{1,2,0:T(1,128)} %broadcast_in_dim.6), calls=%async_computation.5 | async-start | bytes 65536 | tf_op jit(solution)/shard_map/all_to_all | solution.py:32
  195.0 26.7 %all-gather.7.cloned.1.call-done = bf16[128,4096]{1,0:T(8,128)(2,1)} async-done(((bf16[128,256]{1,0:T(8,128)(2,1)}), bf16[128,4096]{1,0:T(8,128)(2,1)}) %all-gather.7.cloned.1.call-update) | async-done | bytes 1048592 | tf_op jit(solution)/shard_map/all_gather | solution.py:11
  221.7 1.3 slice_bitcast_fusion
  223.9 7.9 %all-to-all-start.1 = ((bf16[64,32,128]{2,0,1:T(8,128)(2,1)}), bf16[64,32,128]{2,0,1:T(8,128)(2,1)S(1)}, u32[]{:S(2)}, u32[]{:S(2)}) async-start(bf16[64,32,128]{2,0,1:T(8,128)(2,1)} %bitcast.100), calls=%async_computation.1 | async-start | bytes 1048576 | tf_op jit(solution)/shard_map/all_to_all | solution.py:75
  231.9 17.8 %all-to-all-done.1 = bf16[64,32,128]{2,0,1:T(8,128)(2,1)S(1)} async-done(((bf16[64,32,128]{2,0,1:T(8,128)(2,1)}), bf16[64,32,128]{2,0,1:T(8,128)(2,1)S(1)}, u32[]{:S(2)}, u32[]{:S(2)}) %all-to-all-start.1) | async-done | bytes 524320 | tf_op jit(solution)/shard_map/all_to_all | solution.py:75
  249.7 1.1 broadcast_in_dim.7
  250.8 4.7 %all-to-all-start.6 = ((bf16[32,256,64]{1,2,0:T(8,128)(2,1)}), bf16[32,256,64]{1,2,0:T(8,128)(2,1)S(1)}, u32[]{:S(2)}, u32[]{:S(2)}) async-start(bf16[32,256,64]{1,2,0:T(8,128)(2,1)} %broadcast_in_dim.7), calls=%async_computation.6 | async-start | bytes 2097152 | tf_op jit(solution)/shard_map/all_to_all | solution.py:32
  256.5 27.6 %all-to-all-done.6 = bf16[32,256,64]{1,2,0:T(8,128)(2,1)S(1)} async-done(((bf16[32,256,64]{1,2,0:T(8,128)(2,1)}), bf16[32,256,64]{1,2,0:T(8,128)(2,1)S(1)}, u32[]{:S(2)}, u32[]{:S(2)}) %all-to-all-start.6) | async-done | bytes 1048608 | tf_op jit(solution)/shard_map/all_to_all | solution.py:32
  284.1 5.0 %all-to-all-start.3 = ((bf16[64,32,128]{2,0,1:T(8,128)(2,1)}), bf16[64,32,128]{2,0,1:T(8,128)(2,1)S(1)}, u32[]{:S(2)}, u32[]{:S(2)}) async-start(bf16[64,32,128]{2,0,1:T(8,128)(2,1)} %bitcast.98), calls=%async_computation.3 | async-start | bytes 1048576 | tf_op jit(solution)/shard_map/all_to_all | solution.py:76
  289.2 31.4 %all-gather.1 = bf16[1,128,2048]{2,1,0:T(8,128)(2,1)S(1)} all-gather(bf16[1,128,128]{2,1,0:T(8,128)(2,1)S(1)} %get-tuple-element.27), channel_id=3, replica_groups=mesh['gr'=2,'fs'=32,'tp'=8] {'gr','tp'}, dimensions={2}, use_global_device_ids=true | all-gather | bytes 557056 | tf_op jit(solution)/shard_map/all_gather | solution.py:72
  320.5 1.5 convolution_bitcast_fusion.1
  322.1 1.8 convolution_convert_fusion
  323.9 1.5 copy.34
  325.4 42.0 %all_to_all.95 = bf16[32,256,64]{1,2,0:T(8,128)(2,1)S(1)} all-to-all(bf16[32,256,64]{1,2,0:T(8,128)(2,1)S(1)} %bitcast.107), channel_id=1, replica_groups=mesh['gr'=2,'fs'=32,'tp'=8] {'fs'}, dimensions={0} | all-to-all | bytes 2097152 | tf_op jit(solution)/shard_map/all_to_all | solution.py:26
  367.5 1.1 broadcast_in_dim.8
  368.6 5.0 %all-to-all-start.8 = ((bf16[32,256,64]{1,2,0:T(8,128)(2,1)}), bf16[32,256,64]{1,2,0:T(8,128)(2,1)S(1)}, u32[]{:S(2)}, u32[]{:S(2)}) async-start(bf16[32,256,64]{1,2,0:T(8,128)(2,1)} %broadcast_in_dim.8), calls=%async_computation.8 | async-start | bytes 2097152 | tf_op jit(solution)/shard_map/all_to_all | solution.py:32
  373.6 1.1 pad_maximum_fusion.2
  374.7 1.1 pad_maximum_fusion.1
  375.7 1.1 pad_maximum_fusion
  376.8 25.3 %all-to-all-done.8 = bf16[32,256,64]{1,2,0:T(8,128)(2,1)S(1)} async-done(((bf16[32,256,64]{1,2,0:T(8,128)(2,1)}), bf16[32,256,64]{1,2,0:T(8,128)(2,1)S(1)}, u32[]{:S(2)}, u32[]{:S(2)}) %all-to-all-start.8) | async-done | bytes 1048608 | tf_op jit(solution)/shard_map/all_to_all | solution.py:32
  402.1 1.4 copy.35
  (39 shorter events, 10.5 us)
Async XLA Ops:
  7.2 70.9 %all-gather.5.cloned.1.call-start = ((), (), s32[]{:S(2)}) async-start(), calls=%async_computation.9 | async-start | bytes 1114112 | tf_op jit(solution)/shard_map/all_gather | solution.py:11
  80.3 25.8 %all-to-all-start = ((bf16[64,32,128]{2,0,1:T(8,128)(2,1)}), bf16[64,32,128]{2,0,1:T(8,128)(2,1)S(1)}, u32[]{:S(2)}, u32[]{:S(2)}) async-start(bf16[64,32,128]{2,0,1:T(8,128)(2,1)} %bitcast.101), calls=%async_computation | async-start | bytes 1048576 | tf_op jit(solution)/shard_map/all_to_all | solution.py:75
  89.7 21.5 %copy-start.4 = (f32[2,128,128]{2,1,0:T(8,128)S(1)}, f32[2,128,128]{2,1,0:T(8,128)}, u32[]{:S(2)}) copy-start(f32[2,128,128]{2,1,0:T(8,128)} %param.9) | copy-start | bytes 393220
  106.1 36.4 %copy-start = (bf16[64,32,128]{2,0,1:T(8,128)(2,1)}, bf16[64,32,128]{2,0,1:T(8,128)(2,1)S(1)}, u32[]{:S(2)}) copy-start(bf16[64,32,128]{2,0,1:T(8,128)(2,1)S(1)} %all-to-all-done) | copy-start | bytes 1572868
  106.1 36.4 %all-to-all-start.2 = ((bf16[64,32,128]{2,0,1:T(8,128)(2,1)}), bf16[64,32,128]{2,0,1:T(8,128)(2,1)S(1)}, u32[]{:S(2)}, u32[]{:S(2)}) async-start(bf16[64,32,128]{2,0,1:T(8,128)(2,1)} %bitcast.99), calls=%async_computation.2 | async-start | bytes 1048576 | tf_op jit(solution)/shard_map/all_to_all | solution.py:76
  144.7 42.5 %all-to-all-start.4 = ((bf16[32,256,64]{1,2,0:T(8,128)(2,1)}), bf16[32,256,64]{1,2,0:T(8,128)(2,1)S(1)}, u32[]{:S(2)}, u32[]{:S(2)}) async-start(bf16[32,256,64]{1,2,0:T(8,128)(2,1)} %bitcast.105), calls=%async_computation.4 | async-start | bytes 2097152 | tf_op jit(solution)/shard_map/all_to_all | solution.py:26
  158.1 63.6 %all-gather.7.cloned.1.call-start = ((), (), s32[]{:S(2)}) async-start(), calls=%async_computation.10 | async-start | bytes 1114112 | tf_op jit(solution)/shard_map/all_gather | solution.py:11
  188.9 35.0 %all-to-all-start.5 = ((f32[32,256,1]{1,2,0:T(1,128)}), f32[32,256,1]{1,2,0:T(1,128)S(1)}, u32[]{:S(2)}, u32[]{:S(2)}) async-start(f32[32,256,1]{1,2,0:T(1,128)} %broadcast_in_dim.6), calls=%async_computation.5 | async-start | bytes 65536 | tf_op jit(solution)/shard_map/all_to_all | solution.py:32
  223.9 25.8 %all-to-all-start.1 = ((bf16[64,32,128]{2,0,1:T(8,128)(2,1)}), bf16[64,32,128]{2,0,1:T(8,128)(2,1)S(1)}, u32[]{:S(2)}, u32[]{:S(2)}) async-start(bf16[64,32,128]{2,0,1:T(8,128)(2,1)} %bitcast.100), calls=%async_computation.1 | async-start | bytes 1048576 | tf_op jit(solution)/shard_map/all_to_all | solution.py:75
  249.7 6.8 %copy-start.2 = (bf16[64,32,128]{2,0,1:T(8,128)(2,1)}, bf16[64,32,128]{2,0,1:T(8,128)(2,1)S(1)}, u32[]{:S(2)}) copy-start(bf16[64,32,128]{2,0,1:T(8,128)(2,1)S(1)} %all-to-all-done.1) | copy-start | bytes 1572868
  250.8 33.3 %all-to-all-start.6 = ((bf16[32,256,64]{1,2,0:T(8,128)(2,1)}), bf16[32,256,64]{1,2,0:T(8,128)(2,1)S(1)}, u32[]{:S(2)}, u32[]{:S(2)}) async-start(bf16[32,256,64]{1,2,0:T(8,128)(2,1)} %broadcast_in_dim.7), calls=%async_computation.6 | async-start | bytes 2097152 | tf_op jit(solution)/shard_map/all_to_all | solution.py:32
  284.1 38.0 %all-to-all-start.3 = ((bf16[64,32,128]{2,0,1:T(8,128)(2,1)}), bf16[64,32,128]{2,0,1:T(8,128)(2,1)S(1)}, u32[]{:S(2)}, u32[]{:S(2)}) async-start(bf16[64,32,128]{2,0,1:T(8,128)(2,1)} %bitcast.98), calls=%async_computation.3 | async-start | bytes 1048576 | tf_op jit(solution)/shard_map/all_to_all | solution.py:76
  368.6 33.5 %all-to-all-start.8 = ((bf16[32,256,64]{1,2,0:T(8,128)(2,1)}), bf16[32,256,64]{1,2,0:T(8,128)(2,1)S(1)}, u32[]{:S(2)}, u32[]{:S(2)}) async-start(bf16[32,256,64]{1,2,0:T(8,128)(2,1)} %broadcast_in_dim.8), calls=%async_computation.8 | async-start | bytes 2097152 | tf_op jit(solution)/shard_map/all_to_all | solution.py:32
  373.6 2.1 copy-start.1
  373.6 2.1 copy-start.3
Sparse Core Ops, SparseCore 0:
  11.7 66.3 all-gather.4
  162.6 59.0 all-gather.6
where the time goes:
time: 411 us; the launch traced here: 410 us
  waiting for transfers between devices  208 us (51%)
  blocking collectives  104 us (25%)
  starting transfers between devices  54.7 us (13%)
  local copies, waits for them, and re-layouts  15.6 us (4%)
  between operations  14.3 us (3%)
  other arithmetic  8.55 us (2%)
  matrix products  4.65 us (1%)
    all_gather x2, waiting for transfers between devices, side_by_side(): lax.all_gather(both, axis, axis=dim, tiled=True)  95.2 us
    all_gather x2, blocking collectives, per_device(): lax.all_gather(down_bf, ('gr', 'tp'), axis=1, tiled=True)  62.2 us
    all_to_all x3, waiting for transfers between devices, from_everyone(): lax.all_to_all(jnp.broadcast_to(value[None], (count, *value.shape)), axis...  52.9 us
    all_to_all x1, blocking collectives, sum_at_owner(): tiles = lax.all_to_all(in_blocks(value, dim, count), axis, 0, 0, tiled=True)  42 us
    all_to_all x2, waiting for transfers between devices, per_device(): lax.all_to_all(gate_all, 'fs', split_axis=1, concat_axis=0, tiled=True)  33.3 us
    all_to_all x1, waiting for transfers between devices, sum_at_owner(): tiles = lax.all_to_all(in_blocks(value, dim, count), axis, 0, 0, tiled=True)  26.9 us
    all_to_all x3, starting transfers between devices, from_everyone(): lax.all_to_all(jnp.broadcast_to(value[None], (count, *value.shape)), axis...  15.8 us
    all_to_all x2, starting transfers between devices, per_device(): lax.all_to_all(gate_all, 'fs', split_axis=1, concat_axis=0, tiled=True)  15.7 us
  transfers between devices with their start and end apart: 10, of which 7 were waited for; matrix products, arithmetic and copies ran while one was open for 4% of the time, Pallas kernels for 0%

commit v1 on v0

v1 whole, which is shorter than its diff:
```python
import jax
import jax.numpy as jnp
from jax import lax
from jax.sharding import Mesh
from jax.sharding import PartitionSpec as P

norm_eps = 1e-06
bf16 = jnp.bfloat16
f32 = jnp.float32

AXES = ("gr", "zl", "yh", "yl", "x", "core")
SIZES = (2, 4, 4, 2, 4, 2)
FS = ("zl", "yh", "yl")
GT = ("gr", "x", "core")


def device(gr, fs, tp):
    return gr * 256 + fs * 8 + tp


def weight_moves(k):
    moves = []
    for gr in range(2):
        for fs in range(32):
            for tp in range(8):
                s = (fs >> 1) & 1
                to = device(s ^ k, 2 * (8 * gr + tp) + (fs & 1), fs >> 2)
                moves.append((device(gr, fs, tp), to))
    return moves


def down_moves(k):
    moves = []
    for gr in range(2):
        for fs in range(32):
            for tp in range(8):
                b = fs & 1
                moves.append((device(gr, fs, tp), device(b ^ k, (fs & ~1) + gr, tp)))
    return moves


def in_order(first, second, swapped):
    return jnp.where(swapped, second, first), jnp.where(swapped, first, second)


def to_everyone(value, axes, count):
    return lax.all_to_all(
        jnp.broadcast_to(value[None], (count, *value.shape)), axes, 0, 0, tiled=True
    )


def weights_for_sampling(norm_gain, gate_weight, up_weight, down_weight):
    gain = norm_gain[:, :, None]
    gate = (gain * gate_weight).astype(bf16)
    up = (gain * up_weight).astype(bf16)
    block = jnp.stack([gate, up]).reshape(256, 256)
    down = down_weight.astype(bf16).reshape(256, 128)
    swapped = lax.axis_index("gr") == 1
    got = [lax.ppermute(block, AXES, weight_moves(k)) for k in range(2)]
    rows = in_order(*got, swapped)
    got = [lax.ppermute(down, AXES, down_moves(k)) for k in range(2)]
    down_rows = in_order(*got, swapped)
    halves = []
    for b in range(2):
        cols = slice(128 * b, 128 * b + 128)
        halves.append(jnp.concatenate([rows[0][:, cols], rows[1][:, cols], down_rows[b]], axis=0))
    sends = jnp.broadcast_to(jnp.stack(halves)[:, None], (2, 4, 768, 128)).reshape(8, 768, 128)
    got = lax.all_to_all(sends, ("yl", "x"), 0, 0, tiled=True)
    got = to_everyone(got, "core", 2)
    got = got.reshape(2, 2, 4, 768, 128)
    gu = got[:, :, :, :512].reshape(2, 2, 4, 2, 2, 2, 64, 128)
    gu = gu.transpose(4, 5, 2, 0, 3, 1, 6, 7).reshape(2, 2, 2048, 128)
    dn = got[:, :, :, 512:].reshape(2, 2, 4, 2, 128, 128)
    dn = dn.transpose(3, 4, 1, 2, 0, 5).reshape(2, 128, 2048)
    return gu[0], gu[1], dn


def normalised(stream):
    return (
        stream * lax.rsqrt(jnp.mean(stream * stream, axis=-1, keepdims=True) + norm_eps)
    ).astype(bf16)


def per_device(prompt, norm_gain, gate_weight, up_weight, down_weight):
    gates, ups, downs = weights_for_sampling(norm_gain, gate_weight, up_weight, down_weight)
    tokens, width = prompt.shape[1:]
    normed = normalised(prompt[0].astype(f32))
    count = tokens // 32
    mine = lax.dynamic_slice_in_dim(prompt[0], lax.axis_index(FS) * count, count, 0).astype(f32)
    for k in range(2):
        gate_act = jnp.dot(normed, gates[k], preferred_element_type=f32)
        up_act = jnp.dot(normed, ups[k], preferred_element_type=f32)
        hidden = (jax.nn.silu(gate_act) * up_act).astype(bf16)
        part = jnp.dot(hidden, downs[k], preferred_element_type=f32).astype(bf16)
        parts = lax.all_to_all(part.reshape(32, count, width), FS, 0, 0, tiled=True)
        mine = mine + 0.5 * jnp.sum(parts.astype(f32), axis=0)
        sent = normalised(mine) if k == 0 else mine.astype(bf16)
        normed = to_everyone(sent, FS, 32).reshape(tokens, width)
    return gates, ups, downs, normed[None]


def solution(mesh):
    fine = Mesh(mesh.devices.reshape(SIZES), AXES)
    in_specs = (P(GT, None, None), P(None, FS), P(None, FS, GT), P(None, FS, GT), P(None, FS, GT))
    out_specs = (P(None, None, FS), P(None, None, FS), P(None, FS, None), P(GT, None, None))
    return jax.shard_map(
        per_device, mesh=fine, in_specs=in_specs, out_specs=out_specs, check_vma=False
    )
```

time: 411 us -> 246 us (0.60)
  the two profiles are of different devices: /device:TPU:8 before, /device:TPU:2 now
where the time goes in v1:
time: 246 us; the launch traced here: 244 us
  waiting for transfers between devices  107 us (43%)
  starting transfers between devices  63 us (26%)
  blocking collectives  39.8 us (16%)
  local copies, waits for them, and re-layouts  20.4 us (8%)
  matrix products  8.21 us (3%)
  other arithmetic  5.21 us (2%)
    all_to_all x2, waiting for transfers between devices, to_everyone(): lax.all_to_all(jnp.broadcast_to(value[None], (count, *value.shape)), axes...  51 us
    all_to_all x1, blocking collectives, per_device(): parts = lax.all_to_all(part.reshape(32, count, width), FS, 0, 0, tiled=True)  33.5 us
    all_to_all x1, waiting for transfers between devices, per_device(): parts = lax.all_to_all(part.reshape(32, count, width), FS, 0, 0, tiled=True)  29.5 us
    all_to_all x1, starting transfers between devices, per_device(): parts = lax.all_to_all(part.reshape(32, count, width), FS, 0, 0, tiled=True)  17.6 us
    all_to_all x1, waiting for transfers between devices, weights_for_sampling(): got = lax.all_to_all(sends, ('yl', 'x'), 0, 0, tiled=True)  15.4 us
    all_to_all x1, starting transfers between devices, weights_for_sampling(): got = lax.all_to_all(sends, ('yl', 'x'), 0, 0, tiled=True)  13.9 us
    ppermute x2, starting transfers between devices, weights_for_sampling(): got = [lax.ppermute(down, AXES, down_moves(k)) for k in range(2)]  11.6 us
    ppermute x2, starting transfers between devices, weights_for_sampling(): got = [lax.ppermute(block, AXES, weight_moves(k)) for k in range(2)]  11.2 us
  transfers between devices with their start and end apart: 8, of which 6 were waited for; matrix products, arithmetic and copies ran while one was open for 4% of the time, Pallas kernels for 0%

profile of v1, /device:TPU:2, one launch (start us, length us, event | category | flops | bytes accessed | tf_op | source)
XLA Modules:
  0.0 244.5 jit_solution(15048522488043201515)
XLA Ops:
  1.5 10.9 %collective-permute-start.2 = (bf16[256,128]{1,0:T(8,128)(2,1)S(1)}, bf16[256,128]{1,0:T(8,128)(2,1)S(1)}, u32[]{:S(2)}, u32[]{:S(2)}) collective-permute-start(bf16[256,128]{1,0:T(8,128)(2,1)S(1)} %bitcast.95), channel_id=1, source_target_pairs={{0,256},{1,257},{2,258},{3,259},{4,260},{5,261},{6,262},{7,263},{8... | collective-permute-start | bytes 196616 | tf_op jit(solution)/shard_map/ppermute | solution.py:61
  13.1 1.1 fusion.28
  14.2 9.1 %collective-permute-start = (bf16[256,256]{1,0:T(8,128)(2,1)S(1)}, bf16[256,256]{1,0:T(8,128)(2,1)S(1)}, u32[]{:S(2)}, u32[]{:S(2)}) collective-permute-start(bf16[256,256]{1,0:T(8,128)(2,1)S(1)} %bitcast.93), channel_id=1, source_target_pairs={{0,256},{1,272},{2,288},{3,304},{4,320},{5,336},{6,352},{7,368},{8... | collective-permute-start | bytes 393224 | tf_op jit(solution)/shard_map/ppermute | solution.py:59
  23.3 2.1 collective-permute-start.1
  25.8 10.7 %collective-permute-done.1 = bf16[256,256]{1,0:T(8,128)(2,1)S(1)} collective-permute-done((bf16[256,256]{1,0:T(8,128)(2,1)S(1)}, bf16[256,256]{1,0:T(8,128)(2,1)S(1)}, u32[]{:S(2)}, u32[]{:S(2)}) %collective-permute-start.1) | collective-permute-done | bytes 131104 | tf_op jit(solution)/shard_map/ppermute | solution.py:59
  36.7 1.4 broadcast_in_dim.12
  38.1 13.9 %all-to-all-start = ((bf16[8,768,128]{2,1,0:T(8,128)(2,1)}), bf16[8,768,128]{2,1,0:T(8,128)(2,1)S(1)}, u32[]{:S(2)}, u32[]{:S(2)}) async-start(bf16[8,768,128]{2,1,0:T(8,128)(2,1)} %bitcast.6), calls=%async_computation | async-start | bytes 3145728 | tf_op jit(solution)/shard_map/all_to_all | solution.py:68
  52.3 15.4 %all-to-all-done = bf16[8,768,128]{2,1,0:T(8,128)(2,1)S(1)} async-done(((bf16[8,768,128]{2,1,0:T(8,128)(2,1)}), bf16[8,768,128]{2,1,0:T(8,128)(2,1)S(1)}, u32[]{:S(2)}, u32[]{:S(2)}) %all-to-all-start) | async-done | bytes 1572896 | tf_op jit(solution)/shard_map/all_to_all | solution.py:68
  68.3 6.3 %all_to_all.30 = bf16[2,8,768,128]{3,2,1,0:T(8,128)(2,1)S(1)} all-to-all(bf16[2,8,768,128]{3,2,1,0:T(8,128)(2,1)S(1)} %broadcast_in_dim.13), channel_id=1, replica_groups=mesh['gr'=2,'zl'=4,'yh'=4,'yl'=2,'x'=4,'core'=2] {'core'}, dimensions={0} | all-to-all | bytes 6291456 | tf_op jit(solution)/shard_map/all_to_all | solution.py:47
  74.7 1.0 slice.75
  75.8 1.2 fusion.37
  78.7 1.6 copy.13
  80.3 1.0 fusion.39
  81.4 0.9 copy-done.3
  82.9 3.3 %fusion = bf16[32,8,2048]{2,1,0:T(8,128)(2,1)} fusion(bf16[128,2048]{0,1:T(8,128)(2,1)} %bitcast.89, bf16[2048,128]{1,0:T(8,128)(2,1)} %bitcast.88, bf16[1,256,2048]{2,1,0:T(8,128)(2,1)} %param.5, f32[256]{0:T(256)S(1)} %add_rsqrt_fusion, f32[256,128]{1,0:T(8,128)S(1)} %fusion.13), kind=kOutput, calls=%fused_computation.4 | convolution fusion | flops 270729216 | bytes 3277824 | tf_op jit(solution)/shard_map/dot_general | solution.py:94
  86.3 17.6 %all-to-all-start.2 = ((bf16[32,8,2048]{2,1,0:T(8,128)(2,1)}), bf16[32,8,2048]{2,1,0:T(8,128)(2,1)S(1)}, u32[]{:S(2)}, u32[]{:S(2)}) async-start(bf16[32,8,2048]{2,1,0:T(8,128)(2,1)} %fusion), calls=%async_computation.2 | async-start | bytes 2097152 | tf_op jit(solution)/shard_map/all_to_all | solution.py:95
  103.9 29.5 %all-to-all-done.2 = bf16[32,8,2048]{2,1,0:T(8,128)(2,1)S(1)} async-done(((bf16[32,8,2048]{2,1,0:T(8,128)(2,1)}), bf16[32,8,2048]{2,1,0:T(8,128)(2,1)S(1)}, u32[]{:S(2)}, u32[]{:S(2)}) %all-to-all-start.2) | async-done | bytes 1048608 | tf_op jit(solution)/shard_map/all_to_all | solution.py:95
  135.2 1.1 broadcast_in_dim.15
  136.3 4.3 %all-to-all-start.3 = ((bf16[32,8,2048]{2,1,0:T(8,128)(2,1)}), bf16[32,8,2048]{2,1,0:T(8,128)(2,1)S(1)}, u32[]{:S(2)}, u32[]{:S(2)}) async-start(bf16[32,8,2048]{2,1,0:T(8,128)(2,1)} %broadcast_in_dim.15), calls=%async_computation.3 | async-start | bytes 2097152 | tf_op jit(solution)/shard_map/all_to_all | solution.py:47
  140.7 1.9 copy.16
  142.6 1.9 copy.17
  144.5 25.4 %all-to-all-done.3 = bf16[32,8,2048]{2,1,0:T(8,128)(2,1)S(1)} async-done(((bf16[32,8,2048]{2,1,0:T(8,128)(2,1)}), bf16[32,8,2048]{2,1,0:T(8,128)(2,1)S(1)}, u32[]{:S(2)}, u32[]{:S(2)}) %all-to-all-start.3) | async-done | bytes 1048608 | tf_op jit(solution)/shard_map/all_to_all | solution.py:47
  169.9 1.5 fusion.9
  171.4 2.9 %fusion.1 = bf16[32,8,2048]{2,1,0:T(8,128)(2,1)} fusion(bf16[128,2048]{0,1:T(8,128)(2,1)} %bitcast.86, bf16[2048,128]{1,0:T(8,128)(2,1)} %bitcast.85, bf16[32,8,2048]{2,1,0:T(8,128)(2,1)S(1)} %all-to-all-done.3, f32[256,128]{1,0:T(8,128)S(1)} %fusion.9), kind=kOutput, calls=%fused_computation.5 | convolution fusion | flops 269156352 | bytes 3276800 | tf_op jit(solution)/shard_map/dot_general | solution.py:94
  174.3 33.5 %all_to_all.31 = bf16[32,8,2048]{2,1,0:T(8,128)(2,1)S(1)} all-to-all(bf16[32,8,2048]{2,1,0:T(8,128)(2,1)} %fusion.1), channel_id=1, replica_groups=mesh['gr'=2,'zl'=4,'yh'=4,'yl'=2,'x'=4,'core'=2] {'zl','yh','yl'}, dimensions={0} | all-to-all | bytes 2097152 | tf_op jit(solution)/shard_map/all_to_all | solution.py:95
  208.8 1.1 broadcast_in_dim.17
  209.9 4.4 %all-to-all-start.5 = ((bf16[32,8,2048]{2,1,0:T(8,128)(2,1)}), bf16[32,8,2048]{2,1,0:T(8,128)(2,1)S(1)}, u32[]{:S(2)}, u32[]{:S(2)}) async-start(bf16[32,8,2048]{2,1,0:T(8,128)(2,1)} %broadcast_in_dim.17), calls=%async_computation.5 | async-start | bytes 2097152 | tf_op jit(solution)/shard_map/all_to_all | solution.py:47
  214.5 1.0 copy.11
  215.6 1.0 copy.12
  216.6 1.3 copy.18
  217.9 25.6 %all-to-all-done.5 = bf16[32,8,2048]{2,1,0:T(8,128)(2,1)S(1)} async-done(((bf16[32,8,2048]{2,1,0:T(8,128)(2,1)}), bf16[32,8,2048]{2,1,0:T(8,128)(2,1)S(1)}, u32[]{:S(2)}, u32[]{:S(2)}) %all-to-all-start.5) | async-done | bytes 1048608 | tf_op jit(solution)/shard_map/all_to_all | solution.py:47
  243.5 1.0 copy.20
  (35 shorter events, 8.5 us)
Async XLA Ops:
  1.5 23.9 %collective-permute-start.2 = (bf16[256,128]{1,0:T(8,128)(2,1)S(1)}, bf16[256,128]{1,0:T(8,128)(2,1)S(1)}, u32[]{:S(2)}, u32[]{:S(2)}) collective-permute-start(bf16[256,128]{1,0:T(8,128)(2,1)S(1)} %bitcast.95), channel_id=1, source_target_pairs={{0,256},{1,257},{2,258},{3,259},{4,260},{5,261},{6,262},{7,263},{8... | collective-permute-start | bytes 196616 | tf_op jit(solution)/shard_map/ppermute | solution.py:61
  12.5 13.0 %collective-permute-start.3 = (bf16[256,128]{1,0:T(8,128)(2,1)S(1)}, bf16[256,128]{1,0:T(8,128)(2,1)S(1)}, u32[]{:S(2)}, u32[]{:S(2)}) collective-permute-start(bf16[256,128]{1,0:T(8,128)(2,1)S(1)} %bitcast.96), channel_id=1, source_target_pairs={{0,0},{1,1},{2,2},{3,3},{4,4},{5,5},{6,6},{7,7},{8,256},{9,257},{1... | collective-permute-start | bytes 196616 | tf_op jit(solution)/shard_map/ppermute | solution.py:61
  14.2 11.6 %collective-permute-start = (bf16[256,256]{1,0:T(8,128)(2,1)S(1)}, bf16[256,256]{1,0:T(8,128)(2,1)S(1)}, u32[]{:S(2)}, u32[]{:S(2)}) collective-permute-start(bf16[256,256]{1,0:T(8,128)(2,1)S(1)} %bitcast.93), channel_id=1, source_target_pairs={{0,256},{1,272},{2,288},{3,304},{4,320},{5,336},{6,352},{7,368},{8... | collective-permute-start | bytes 393224 | tf_op jit(solution)/shard_map/ppermute | solution.py:59
  23.3 13.2 %collective-permute-start.1 = (bf16[256,256]{1,0:T(8,128)(2,1)S(1)}, bf16[256,256]{1,0:T(8,128)(2,1)S(1)}, u32[]{:S(2)}, u32[]{:S(2)}) collective-permute-start(bf16[256,256]{1,0:T(8,128)(2,1)S(1)} %bitcast.94), channel_id=1, source_target_pairs={{0,0},{1,16},{2,32},{3,48},{4,64},{5,80},{6,96},{7,112},{8,8},{9,2... | collective-permute-start | bytes 393224 | tf_op jit(solution)/shard_map/ppermute | solution.py:59
  36.7 15.3 %copy-start.2 = (bf16[1,256,2048]{2,1,0:T(8,128)(2,1)S(1)}, bf16[1,256,2048]{2,1,0:T(8,128)(2,1)}, u32[]{:S(2)}) copy-start(bf16[1,256,2048]{2,1,0:T(8,128)(2,1)} %param.5) | copy-start | bytes 3145732
  38.1 29.6 %all-to-all-start = ((bf16[8,768,128]{2,1,0:T(8,128)(2,1)}), bf16[8,768,128]{2,1,0:T(8,128)(2,1)S(1)}, u32[]{:S(2)}, u32[]{:S(2)}) async-start(bf16[8,768,128]{2,1,0:T(8,128)(2,1)} %bitcast.6), calls=%async_computation | async-start | bytes 3145728 | tf_op jit(solution)/shard_map/all_to_all | solution.py:68
  80.3 5.9 %copy-start = (bf16[2,2,4,2,128,128]{4,5,0,2,1,3:T(8,128)(2,1)}, bf16[2,2,4,2,128,128]{4,5,0,2,1,3:T(8,128)(2,1)S(1)}, u32[]{:S(2)}) copy-start(bf16[2,2,4,2,128,128]{4,5,0,2,1,3:T(8,128)(2,1)S(1)} %copy.13) | copy-start | bytes 3145732
  80.3 2.0 copy-start.3
  80.3 2.1 copy-start.4
  86.3 47.1 %all-to-all-start.2 = ((bf16[32,8,2048]{2,1,0:T(8,128)(2,1)}), bf16[32,8,2048]{2,1,0:T(8,128)(2,1)S(1)}, u32[]{:S(2)}, u32[]{:S(2)}) async-start(bf16[32,8,2048]{2,1,0:T(8,128)(2,1)} %fusion), calls=%async_computation.2 | async-start | bytes 2097152 | tf_op jit(solution)/shard_map/all_to_all | solution.py:95
  136.3 33.6 %all-to-all-start.3 = ((bf16[32,8,2048]{2,1,0:T(8,128)(2,1)}), bf16[32,8,2048]{2,1,0:T(8,128)(2,1)S(1)}, u32[]{:S(2)}, u32[]{:S(2)}) async-start(bf16[32,8,2048]{2,1,0:T(8,128)(2,1)} %broadcast_in_dim.15), calls=%async_computation.3 | async-start | bytes 2097152 | tf_op jit(solution)/shard_map/all_to_all | solution.py:47
  209.9 33.6 %all-to-all-start.5 = ((bf16[32,8,2048]{2,1,0:T(8,128)(2,1)}), bf16[32,8,2048]{2,1,0:T(8,128)(2,1)S(1)}, u32[]{:S(2)}, u32[]{:S(2)}) async-start(bf16[32,8,2048]{2,1,0:T(8,128)(2,1)} %broadcast_in_dim.17), calls=%async_computation.5 | async-start | bytes 2097152 | tf_op jit(solution)/shard_map/all_to_all | solution.py:47
  214.5 2.1 copy-start.1

commit v2 on v1

v2 whole, which is shorter than its diff:
```python
import jax
import jax.numpy as jnp
from jax import lax
from jax.experimental import pallas as pl
from jax.experimental.pallas import tpu as pltpu
from jax.sharding import Mesh
from jax.sharding import PartitionSpec as P

norm_eps = 1e-06
bf16 = jnp.bfloat16
f32 = jnp.float32

AXES = ("gr", "zl", "yh", "yl", "x", "core")
SIZES = (2, 4, 4, 2, 4, 2)
FS = ("zl", "yh", "yl")
GT = ("gr", "x", "core")
SWAP = [(0, 1), (1, 0)]


def device(gr, fs, tp):
    return gr * 256 + fs * 8 + tp


def everyone():
    return [(gr, fs, tp) for gr in range(2) for fs in range(32) for tp in range(8)]


def weight_moves(k):
    moves = []
    for gr, fs, tp in everyone():
        to = device(((fs >> 1) & 1) ^ k, 2 * (8 * gr + tp) + (fs & 1), fs >> 2)
        moves.append((device(gr, fs, tp), to))
    return moves


def in_order(first, second, swapped):
    return jnp.where(swapped, second, first), jnp.where(swapped, first, second)


def halves_to_all(blocks):
    rows = blocks[0].shape[0]
    sends = jnp.broadcast_to(jnp.stack(blocks)[None], (4, 2, rows, 128)).reshape(8, rows, 128)
    return lax.all_to_all(sends, ("x", "yl"), 0, 0, tiled=True)


def columns(rows, b):
    return [r[:, 128 * b : 128 * b + 128] for r in rows]


def gather_rows(core, own, other, both):
    mine = core == 0
    for x in range(4):
        for b in range(2):
            for s in range(2):
                mn = own[2 * x + b, 128 * s : 128 * s + 128]
                ot = other[2 * x + b, 128 * s : 128 * s + 128]
                for c in range(2):
                    line = jnp.where(mine, mn, ot) if c == 0 else jnp.where(mine, ot, mn)
                    at = 64 * (8 * x + 4 * c + 2 * s + b)
                    both[at : at + 64, :128] = line[:64]
                    both[at : at + 64, 128:] = line[64:]


def up_call(late, stream, own, other):
    def part_of(stream, z):
        if late:
            return stream[z // 2, :, 512 * (z % 2) : 512 * (z % 2) + 512].astype(f32)
        return stream[:, 512 * z : 512 * z + 512].astype(f32)

    def body(stream, own, other, gate, up, hidden, both):
        gather_rows(lax.axis_index("core"), own, other, both)
        gate[...] = both[:, :128]
        up[...] = both[:, 128:]
        squares = jnp.zeros((256, 1), f32)
        for z in range(4):
            part = part_of(stream, z)
            squares = squares + jnp.sum(part * part, axis=1, keepdims=True)
        scale = lax.rsqrt(squares * (1.0 / 2048) + norm_eps)
        act = jnp.zeros((256, 256), f32)
        for z in range(4):
            normed = (part_of(stream, z) * scale).astype(bf16)
            act = act + jnp.dot(normed, both[512 * z : 512 * z + 512], preferred_element_type=f32)
        gate_act, up_act = act[:, :128], act[:, 128:]
        hidden[...] = (gate_act / (1.0 + jnp.exp(-gate_act)) * up_act).astype(bf16)

    return pl.pallas_call(
        body,
        out_shape=(
            jax.ShapeDtypeStruct((2048, 128), bf16),
            jax.ShapeDtypeStruct((2048, 128), bf16),
            jax.ShapeDtypeStruct((256, 128), bf16),
        ),
        scratch_shapes=[pltpu.VMEM((2048, 256), bf16)],
        name="late_up" if late else "early_up",
    )(stream, own, other)


def down_rows_call(own, other):
    def body(own, other, keep, send):
        mine = lax.axis_index("core") == 0
        even = lax.axis_index("yl") == 0
        for x in range(4):
            for k in range(2):
                at = 256 + 128 * k
                mn = [own[2 * x + b, at : at + 128] for b in range(2)]
                ot = [other[2 * x + b, at : at + 128] for b in range(2)]
                for c in range(2):
                    a, b = (mn, ot) if c == 0 else (ot, mn)
                    line = [jnp.where(mine, a[i], b[i]) for i in range(2)]
                    col = 256 * x + 128 * c
                    keep[k, :, col : col + 128] = jnp.where(even, line[0], line[1])
                    send[k, :, col : col + 128] = jnp.where(even, line[1], line[0])

    shape = jax.ShapeDtypeStruct((2, 128, 1024), bf16)
    return pl.pallas_call(body, out_shape=(shape, shape), name="down_rows")(own, other)


def down_call(layer, own, other, keep, send):
    def body(own, other, keep, send, out):
        act = jnp.dot(own[...], keep[layer], preferred_element_type=f32)
        act = act + jnp.dot(other[...], send[layer], preferred_element_type=f32)
        out[...] = act.astype(bf16)

    return pl.pallas_call(
        body, out_shape=jax.ShapeDtypeStruct((256, 1024), bf16), name="down"
    )(own, other, keep, send)


def per_device(prompt, norm_gain, gate_weight, up_weight, down_weight):
    gain = norm_gain[:, :, None]
    gate = (gain * gate_weight).astype(bf16)
    up = (gain * up_weight).astype(bf16)
    high = lax.axis_index("gr") == 1
    rows = []
    for layer in range(2):
        block = jnp.concatenate([gate[layer], up[layer]], axis=0)
        got = [lax.ppermute(block, AXES, weight_moves(k)) for k in range(2)]
        rows.append(in_order(*got, high))
    down = down_weight.astype(bf16).reshape(256, 128)
    downs = in_order(down, lax.ppermute(down, "gr", SWAP), high)
    early = halves_to_all([jnp.concatenate([*columns(rows[0], b), downs[b]]) for b in range(2)])
    early = early, lax.ppermute(early, "core", SWAP)
    late = halves_to_all([jnp.concatenate(columns(rows[1], b)) for b in range(2)])
    late = late, lax.ppermute(late, "core", SWAP)
    keep, send = down_rows_call(*early)
    came = lax.ppermute(send, "yl", SWAP)

    stream = prompt[0]
    yl = lax.axis_index("yl")
    mine = lax.dynamic_slice(
        stream, (lax.axis_index(("zl", "yh")) * 16, yl * 1024), (16, 1024)
    ).astype(f32)
    gates, ups = [], []
    for layer in range(2):
        gate, up, hidden = up_call(layer == 1, stream, *(late if layer else early))
        gates.append(gate)
        ups.append(up)
        part = down_call(layer, hidden, lax.ppermute(hidden, "yl", SWAP), keep, send)
        parts = lax.all_to_all(part.reshape(16, 16, 1024), ("zl", "yh"), 0, 0, tiled=True)
        mine = mine + 0.5 * jnp.sum(parts.astype(f32), axis=0)
        sends = jnp.broadcast_to(mine.astype(bf16)[None], (32, 16, 1024))
        stream = lax.all_to_all(sends, ("yl", "zl", "yh"), 0, 0, tiled=True).reshape(2, 256, 1024)
    mixed = jnp.concatenate(list(stream), axis=1)
    served = jnp.concatenate(in_order(keep, came, yl == 1), axis=2)
    return jnp.stack(gates), jnp.stack(ups), served, mixed[None]


def solution(mesh):
    fine = Mesh(mesh.devices.reshape(SIZES), AXES)
    in_specs = (P(GT, None, None), P(None, FS), P(None, FS, GT), P(None, FS, GT), P(None, FS, GT))
    out_specs = (P(None, None, FS), P(None, None, FS), P(None, FS, None), P(GT, None, None))
    return jax.shard_map(
        per_device, mesh=fine, in_specs=in_specs, out_specs=out_specs, check_vma=False
    )
```

time: 246 us -> 240 us (0.976)
  Pallas kernels: 0 us -> 14.6 us
  local copies, waits for them, and re-layouts: 20.4 us -> 7.59 us
  waiting for transfers between devices: 107 us -> 94.4 us
  matrix products: 8.21 us -> 0 us
  starting transfers between devices: 63 us -> 69.5 us
  blocking collectives: 39.8 us -> 43 us
  other arithmetic: 5.21 us -> 8.18 us
    all_to_all x4, waiting for transfers between devices: 95.9 us -> 49.1 us  [the longest x2 23.8 us: per_device(): lax.all_to_all(sends, ('yl', 'zl', 'yh'), 0, 0, tiled=True)]
    ppermute x4 -> x10, waiting for transfers between devices: 11.1 us -> 45.3 us  [the longest x1 32.1 us: per_device(): came = lax.ppermute(send, 'yl', SWAP)]
    ppermute x4 -> x10, starting transfers between devices: 22.7 us -> 48.4 us  [the longest x4 29.8 us: per_device(): got = [lax.ppermute(block, AXES, weight_moves(k)) for k in range(2)]]
    all_to_all x4, starting transfers between devices: 40.3 us -> 21.1 us  [the longest x2 9.31 us: per_device(): lax.all_to_all(sends, ('yl', 'zl', 'yh'), 0, 0, tiled=True)]
    pallas_call x0 -> x5, Pallas kernels: none -> 14.6 us  [the longest x2 6.77 us: up_call(): pl.pallas_call(body, out_shape=(jax.ShapeDtypeStruct((2048, 128), bf16),...]
    slice x13 -> x4, local copies, waits for them, and re-layouts: 11.2 us -> 0.03 us  [columns(): return [r[:, 128 * b:128 * b + 128] for r in rows]]
    dot_general x4 -> x0, matrix products: 8.21 us -> none  [the longest x2 6.27 us: per_device(): part = jnp.dot(hidden, downs[k], preferred_element_type=f32).astype(bf16)]
    all_to_all x2, blocking collectives: 39.8 us -> 43 us  [the longest x1 22.5 us: per_device(): lax.all_to_all(part.reshape(16, 16, 1024), ('zl', 'yh'), 0, 0, tiled=True)]
  transfers between devices with their start and end apart: 8 -> 14, of which waited for: 6 -> 9; matrix products, arithmetic and copies ran while one was open for 4% -> 2% of each run, Pallas kernels for 0% -> 1%
where the time goes in v2:
time: 240 us; the launch traced here: 238 us
  waiting for transfers between devices  94.4 us (39%)
  starting transfers between devices  69.5 us (29%)
  blocking collectives  43 us (18%)
  Pallas kernels  14.6 us (6%)
  other arithmetic  8.18 us (3%)
  local copies, waits for them, and re-layouts  7.59 us (3%)
    ppermute x1, waiting for transfers between devices, per_device(): came = lax.ppermute(send, 'yl', SWAP)  32.1 us
    ppermute x4, starting transfers between devices, per_device(): got = [lax.ppermute(block, AXES, weight_moves(k)) for k in range(2)]  29.8 us
    all_to_all x2, waiting for transfers between devices, per_device(): lax.all_to_all(sends, ('yl', 'zl', 'yh'), 0, 0, tiled=True)  23.8 us
    all_to_all x1, blocking collectives, per_device(): lax.all_to_all(part.reshape(16, 16, 1024), ('zl', 'yh'), 0, 0, tiled=True)  22.5 us
    all_to_all x1, blocking collectives, halves_to_all(): return lax.all_to_all(sends, ('x', 'yl'), 0, 0, tiled=True)  20.5 us
    all_to_all x1, waiting for transfers between devices, per_device(): lax.all_to_all(part.reshape(16, 16, 1024), ('zl', 'yh'), 0, 0, tiled=True)  19.3 us
    all_to_all x2, starting transfers between devices, per_device(): lax.all_to_all(sends, ('yl', 'zl', 'yh'), 0, 0, tiled=True)  9.31 us
    all_to_all x1, starting transfers between devices, per_device(): lax.all_to_all(part.reshape(16, 16, 1024), ('zl', 'yh'), 0, 0, tiled=True)  7.66 us
  transfers between devices with their start and end apart: 14, of which 9 were waited for; matrix products, arithmetic and copies ran while one was open for 2% of the time, Pallas kernels for 1%

profile of v2, /device:TPU:2, one launch (start us, length us, event | category | flops | bytes accessed | tf_op | source)
XLA Modules:
  0.0 238.3 jit_solution(2644598368047861902)
XLA Ops:
  0.6 1.1 multiply_convert_fusion.1
  1.8 16.1 %collective-permute-start = (bf16[128,256]{1,0:T(8,128)(2,1)S(1)}, bf16[128,256]{1,0:T(8,128)(2,1)S(1)}, u32[]{:S(2)}, u32[]{:S(2)}) collective-permute-start(bf16[128,256]{1,0:T(8,128)(2,1)S(1)} %pad_maximum_fusion.5), channel_id=1, source_target_pairs={{0,256},{1,272},{2,288},{3,304},{4,320},{5,336},{6,352},{7,368},{8... | collective-permute-start | bytes 196616 | tf_op jit(solution)/shard_map/ppermute | solution.py:137
  18.0 1.9 collective-permute-start.1
  19.9 9.8 %collective-permute-start.5 = (bf16[128,256]{1,0:T(8,128)(2,1)S(1)}, bf16[128,256]{1,0:T(8,128)(2,1)S(1)}, u32[]{:S(2)}, u32[]{:S(2)}) collective-permute-start(bf16[128,256]{1,0:T(8,128)(2,1)S(1)} %pad_maximum_fusion.6), channel_id=1, source_target_pairs={{0,256},{1,272},{2,288},{3,304},{4,320},{5,336},{6,352},{7,368},{8... | collective-permute-start | bytes 196616 | tf_op jit(solution)/shard_map/ppermute | solution.py:137
  29.7 1.9 collective-permute-start.6
  32.5 5.2 %collective-permute-start.2 = (bf16[256,128]{1,0:T(8,128)(2,1)S(1)}, bf16[256,128]{1,0:T(8,128)(2,1)S(1)}, u32[]{:S(2)}, u32[]{:S(2)}) collective-permute-start(bf16[256,128]{1,0:T(8,128)(2,1)S(1)} %bitcast.64), channel_id=1, source_target_pairs={{0,256},{256,0},{1,257},{257,1},{2,258},{258,2},{3,259},{259,3},{4... | collective-permute-start | bytes 196616 | tf_op jit(solution)/shard_map/ppermute | solution.py:140
  37.8 4.8 %collective-permute-done.2 = bf16[256,128]{1,0:T(8,128)(2,1)S(1)} collective-permute-done((bf16[256,128]{1,0:T(8,128)(2,1)S(1)}, bf16[256,128]{1,0:T(8,128)(2,1)S(1)}, u32[]{:S(2)}, u32[]{:S(2)}) %collective-permute-start.2) | collective-permute-done | bytes 65568 | tf_op jit(solution)/shard_map/ppermute | solution.py:140
  42.8 20.5 %all_to_all.30.own = bf16[8,512,128]{2,1,0:T(8,128)(2,1)S(1)} all-to-all(bf16[8,512,128]{2,1,0:T(8,128)(2,1)S(1)} %bitcast.53), channel_id=1, replica_groups=mesh['gr'=2,'zl'=4,'yh'=4,'yl'=2,'x'=4,'core'=2] {'x','yl'}, dimensions={0} | all-to-all | bytes 2097152 | tf_op jit(solution)/shard_map/all_to_all | solution.py:43
  63.3 1.9 collective-permute-start.3
  65.2 2.6 %collective-permute-done.3.other = bf16[8,512,128]{2,1,0:T(8,128)(2,1)S(1)} collective-permute-done((bf16[8,512,128]{2,1,0:T(8,128)(2,1)S(1)}, bf16[8,512,128]{2,1,0:T(8,128)(2,1)S(1)}, u32[]{:S(2)}, u32[]{:S(2)}) %collective-permute-start.3) | collective-permute-done | bytes 1048608 | tf_op jit(solution)/shard_map/ppermute | solution.py:142
  68.8 3.5 %early_up.1 = (bf16[2048,128]{1,0:T(8,128)(2,1)}, bf16[2048,128]{1,0:T(8,128)(2,1)}, bf16[256,128]{1,0:T(8,128)(2,1)}) custom-call(bf16[256,2048]{1,0:T(8,128)(2,1)} %bitcast.59, bf16[8,512,128]{2,1,0:T(8,128)(2,1)} %copy-done, bf16[8,512,128]{2,1,0:T(8,128)(2,1)} %copy-done.2), custom_call_target="tpu_custom_call" | custom-call | tf_op jit(solution)/shard_map/early_up/pallas_call | solution.py:86
  72.4 3.1 %collective-permute-start.4 = (bf16[256,128]{1,0:T(8,128)(2,1)}, bf16[256,128]{1,0:T(8,128)(2,1)S(1)}, u32[]{:S(2)}, u32[]{:S(2)}) collective-permute-start(bf16[256,128]{1,0:T(8,128)(2,1)} %get-tuple-element.13.own), channel_id=1, source_target_pairs={{0,8},{8,0},{1,9},{9,1},{2,10},{10,2},{3,11},{11,3},{4,12},{12,4},... | collective-permute-start | bytes 196616 | tf_op jit(solution)/shard_map/ppermute | solution.py:158
  75.4 2.9 %down_rows.1 = (bf16[2,128,1024]{2,1,0:T(8,128)(2,1)}, bf16[2,128,1024]{2,1,0:T(8,128)(2,1)}) custom-call(bf16[8,512,128]{2,1,0:T(8,128)(2,1)} %copy-done, bf16[8,512,128]{2,1,0:T(8,128)(2,1)} %copy-done.2), custom_call_target="tpu_custom_call" | custom-call | tf_op jit(solution)/shard_map/down_rows/pallas_call | solution.py:115
  79.4 2.5 %down.2 = bf16[256,1024]{1,0:T(8,128)(2,1)} custom-call(bf16[256,128]{1,0:T(8,128)(2,1)} %get-tuple-element.13.own, bf16[256,128]{1,0:T(8,128)(2,1)} %copy-done.12, bf16[2,128,1024]{2,1,0:T(8,128)(2,1)} %get-tuple-element.14.keep, bf16[2,128,1024]{2,1,0:T(8,128)(2,1)} %get-tuple-element.15.send), custom_call_target="tpu_custom_call" | custom-call | tf_op jit(solution)/shard_map/down/pallas_call | solution.py:124
  81.8 7.7 %all-to-all-start.1 = ((bf16[16,16,1024]{2,1,0:T(8,128)(2,1)}), bf16[16,16,1024]{2,1,0:T(8,128)(2,1)S(1)}, u32[]{:S(2)}, u32[]{:S(2)}) async-start(bf16[16,16,1024]{2,1,0:T(8,128)(2,1)} %bitcast.55), calls=%async_computation.1 | async-start | bytes 1048576 | tf_op jit(solution)/shard_map/all_to_all | solution.py:159
  89.6 19.3 %all-to-all-done.1 = bf16[16,16,1024]{2,1,0:T(8,128)(2,1)S(1)} async-done(((bf16[16,16,1024]{2,1,0:T(8,128)(2,1)}), bf16[16,16,1024]{2,1,0:T(8,128)(2,1)S(1)}, u32[]{:S(2)}, u32[]{:S(2)}) %all-to-all-start.1) | async-done | bytes 524320 | tf_op jit(solution)/shard_map/all_to_all | solution.py:159
  109.8 4.1 %all-to-all-start.3 = ((bf16[8,256,128]{2,1,0:T(8,128)(2,1)}), bf16[8,256,128]{2,1,0:T(8,128)(2,1)S(1)}, u32[]{:S(2)}, u32[]{:S(2)}) async-start(bf16[8,256,128]{2,1,0:T(8,128)(2,1)} %bitcast.16), calls=%async_computation.3 | async-start | bytes 1048576 | tf_op jit(solution)/shard_map/all_to_all | solution.py:43
  114.7 6.0 %all-to-all-done.3.own = bf16[8,256,128]{2,1,0:T(8,128)(2,1)S(1)} async-done(((bf16[8,256,128]{2,1,0:T(8,128)(2,1)}), bf16[8,256,128]{2,1,0:T(8,128)(2,1)S(1)}, u32[]{:S(2)}, u32[]{:S(2)}) %all-to-all-start.3) | async-done | bytes 524320 | tf_op jit(solution)/shard_map/all_to_all | solution.py:43
  120.7 1.1 broadcast_in_dim.16
  121.9 5.2 %all-to-all-start.2 = ((bf16[32,16,1024]{2,1,0:T(8,128)(2,1)}), bf16[32,16,1024]{2,1,0:T(8,128)(2,1)S(1)}, u32[]{:S(2)}, u32[]{:S(2)}) async-start(bf16[32,16,1024]{2,1,0:T(8,128)(2,1)} %broadcast_in_dim.16), calls=%async_computation.2 | async-start | bytes 2097152 | tf_op jit(solution)/shard_map/all_to_all | solution.py:162
  127.0 1.9 collective-permute-start.7
  129.0 1.9 collective-permute-done.7.other
  130.9 23.8 %all-to-all-done.2 = bf16[32,16,1024]{2,1,0:T(8,128)(2,1)S(1)} async-done(((bf16[32,16,1024]{2,1,0:T(8,128)(2,1)}), bf16[32,16,1024]{2,1,0:T(8,128)(2,1)S(1)}, u32[]{:S(2)}, u32[]{:S(2)}) %all-to-all-start.2) | async-done | bytes 1048608 | tf_op jit(solution)/shard_map/all_to_all | solution.py:162
  155.7 3.2 %late_up.1 = (bf16[2048,128]{1,0:T(8,128)(2,1)}, bf16[2048,128]{1,0:T(8,128)(2,1)}, bf16[256,128]{1,0:T(8,128)(2,1)}) custom-call(bf16[2,256,1024]{2,1,0:T(8,128)(2,1)} %bitcast.54, bf16[8,256,128]{2,1,0:T(8,128)(2,1)} %copy-done.5, bf16[8,256,128]{2,1,0:T(8,128)(2,1)} %copy-done.11), custom_call_target="tpu_custom_call" | custom-call | tf_op jit(solution)/shard_map/late_up/pallas_call | solution.py:86
  158.9 2.9 %collective-permute-start.9 = (bf16[256,128]{1,0:T(8,128)(2,1)}, bf16[256,128]{1,0:T(8,128)(2,1)S(1)}, u32[]{:S(2)}, u32[]{:S(2)}) collective-permute-start(bf16[256,128]{1,0:T(8,128)(2,1)} %get-tuple-element.19.own), channel_id=1, source_target_pairs={{0,8},{8,0},{1,9},{9,1},{2,10},{10,2},{3,11},{11,3},{4,12},{12,4},... | collective-permute-start | bytes 196616 | tf_op jit(solution)/shard_map/ppermute | solution.py:158
  161.8 3.5 %collective-permute-done.9.other = bf16[256,128]{1,0:T(8,128)(2,1)S(1)} collective-permute-done((bf16[256,128]{1,0:T(8,128)(2,1)}, bf16[256,128]{1,0:T(8,128)(2,1)S(1)}, u32[]{:S(2)}, u32[]{:S(2)}) %collective-permute-start.9) | collective-permute-done | bytes 65568 | tf_op jit(solution)/shard_map/ppermute | solution.py:158
  165.9 2.5 %down.3 = bf16[256,1024]{1,0:T(8,128)(2,1)} custom-call(bf16[256,128]{1,0:T(8,128)(2,1)} %get-tuple-element.19.own, bf16[256,128]{1,0:T(8,128)(2,1)} %copy-done.13, bf16[2,128,1024]{2,1,0:T(8,128)(2,1)} %get-tuple-element.14.keep, bf16[2,128,1024]{2,1,0:T(8,128)(2,1)} %get-tuple-element.15.send), custom_call_target="tpu_custom_call" | custom-call | tf_op jit(solution)/shard_map/down/pallas_call | solution.py:124
  168.4 22.5 %all_to_all.31 = bf16[16,16,1024]{2,1,0:T(8,128)(2,1)S(1)} all-to-all(bf16[16,16,1024]{2,1,0:T(8,128)(2,1)} %bitcast.56), channel_id=1, replica_groups=mesh['gr'=2,'zl'=4,'yh'=4,'yl'=2,'x'=4,'core'=2] {'zl','yh'}, dimensions={0} | all-to-all | bytes 1048576 | tf_op jit(solution)/shard_map/all_to_all | solution.py:159
  191.8 1.1 broadcast_in_dim.37
  192.9 4.1 %all-to-all-start.5 = ((bf16[32,16,1024]{2,1,0:T(8,128)(2,1)}), bf16[32,16,1024]{2,1,0:T(8,128)(2,1)S(1)}, u32[]{:S(2)}, u32[]{:S(2)}) async-start(bf16[32,16,1024]{2,1,0:T(8,128)(2,1)} %broadcast_in_dim.37), calls=%async_computation.5 | async-start | bytes 2097152 | tf_op jit(solution)/shard_map/all_to_all | solution.py:162
  197.0 3.7 %collective-permute-start.8 = (bf16[2,128,1024]{2,1,0:T(8,128)(2,1)S(1)}, bf16[2,128,1024]{2,1,0:T(8,128)(2,1)S(1)}, u32[]{:S(2)}, u32[]{:S(2)}) collective-permute-start(bf16[2,128,1024]{2,1,0:T(8,128)(2,1)S(1)} %copy-done.4), channel_id=1, source_target_pairs={{0,8},{8,0},{1,9},{9,1},{2,10},{10,2},{3,11},{11,3},{4,12},{12,4},... | collective-permute-start | bytes 1572872 | tf_op jit(solution)/shard_map/ppermute | solution.py:146
  200.8 32.1 %collective-permute-done.8 = bf16[2,128,1024]{2,1,0:T(8,128)(2,1)S(1)} collective-permute-done((bf16[2,128,1024]{2,1,0:T(8,128)(2,1)S(1)}, bf16[2,128,1024]{2,1,0:T(8,128)(2,1)S(1)}, u32[]{:S(2)}, u32[]{:S(2)}) %collective-permute-start.8) | collective-permute-done | bytes 524320 | tf_op jit(solution)/shard_map/ppermute | solution.py:146
  (63 shorter events, 12.9 us)
Async XLA Ops:
  0.6 42.0 %copy-start.6 = (f32[2,128,128]{2,1,0:T(8,128)S(1)}, f32[2,128,128]{2,1,0:T(8,128)}, u32[]{:S(2)}) copy-start(f32[2,128,128]{2,1,0:T(8,128)} %param.9) | copy-start | bytes 393220
  1.8 35.9 %collective-permute-start = (bf16[128,256]{1,0:T(8,128)(2,1)S(1)}, bf16[128,256]{1,0:T(8,128)(2,1)S(1)}, u32[]{:S(2)}, u32[]{:S(2)}) collective-permute-start(bf16[128,256]{1,0:T(8,128)(2,1)S(1)} %pad_maximum_fusion.5), channel_id=1, source_target_pairs={{0,256},{1,272},{2,288},{3,304},{4,320},{5,336},{6,352},{7,368},{8... | collective-permute-start | bytes 196616 | tf_op jit(solution)/shard_map/ppermute | solution.py:137
  18.0 19.8 %collective-permute-start.1 = (bf16[128,256]{1,0:T(8,128)(2,1)S(1)}, bf16[128,256]{1,0:T(8,128)(2,1)S(1)}, u32[]{:S(2)}, u32[]{:S(2)}) collective-permute-start(bf16[128,256]{1,0:T(8,128)(2,1)S(1)} %pad_maximum_fusion.5), channel_id=1, source_target_pairs={{0,0},{1,16},{2,32},{3,48},{4,64},{5,80},{6,96},{7,112},{8,8},{9,2... | collective-permute-start | bytes 196616 | tf_op jit(solution)/shard_map/ppermute | solution.py:137
  19.9 17.9 %collective-permute-start.5 = (bf16[128,256]{1,0:T(8,128)(2,1)S(1)}, bf16[128,256]{1,0:T(8,128)(2,1)S(1)}, u32[]{:S(2)}, u32[]{:S(2)}) collective-permute-start(bf16[128,256]{1,0:T(8,128)(2,1)S(1)} %pad_maximum_fusion.6), channel_id=1, source_target_pairs={{0,256},{1,272},{2,288},{3,304},{4,320},{5,336},{6,352},{7,368},{8... | collective-permute-start | bytes 196616 | tf_op jit(solution)/shard_map/ppermute | solution.py:137
  29.7 8.1 %collective-permute-start.6 = (bf16[128,256]{1,0:T(8,128)(2,1)S(1)}, bf16[128,256]{1,0:T(8,128)(2,1)S(1)}, u32[]{:S(2)}, u32[]{:S(2)}) collective-permute-start(bf16[128,256]{1,0:T(8,128)(2,1)S(1)} %pad_maximum_fusion.6), channel_id=1, source_target_pairs={{0,0},{1,16},{2,32},{3,48},{4,64},{5,80},{6,96},{7,112},{8,8},{9,2... | collective-permute-start | bytes 196616 | tf_op jit(solution)/shard_map/ppermute | solution.py:137
  32.5 10.1 %collective-permute-start.2 = (bf16[256,128]{1,0:T(8,128)(2,1)S(1)}, bf16[256,128]{1,0:T(8,128)(2,1)S(1)}, u32[]{:S(2)}, u32[]{:S(2)}) collective-permute-start(bf16[256,128]{1,0:T(8,128)(2,1)S(1)} %bitcast.64), channel_id=1, source_target_pairs={{0,256},{256,0},{1,257},{257,1},{2,258},{258,2},{3,259},{259,3},{4... | collective-permute-start | bytes 196616 | tf_op jit(solution)/shard_map/ppermute | solution.py:140
  63.3 4.5 %copy-start = (bf16[8,512,128]{2,1,0:T(8,128)(2,1)}, bf16[8,512,128]{2,1,0:T(8,128)(2,1)S(1)}, u32[]{:S(2)}) copy-start(bf16[8,512,128]{2,1,0:T(8,128)(2,1)S(1)} %all_to_all.30.own) | copy-start | bytes 3145732
  63.3 4.5 %collective-permute-start.3 = (bf16[8,512,128]{2,1,0:T(8,128)(2,1)S(1)}, bf16[8,512,128]{2,1,0:T(8,128)(2,1)S(1)}, u32[]{:S(2)}, u32[]{:S(2)}) collective-permute-start(bf16[8,512,128]{2,1,0:T(8,128)(2,1)S(1)} %all_to_all.30.own), channel_id=1, source_target_pairs={{0,1},{1,0},{2,3},{3,2},{4,5},{5,4},{6,7},{7,6},{8,9},{9,8},{10,11... | collective-permute-start | bytes 3145736 | tf_op jit(solution)/shard_map/ppermute | solution.py:142
  67.8 1.0 copy-start.2
  72.4 6.4 %collective-permute-start.4 = (bf16[256,128]{1,0:T(8,128)(2,1)}, bf16[256,128]{1,0:T(8,128)(2,1)S(1)}, u32[]{:S(2)}, u32[]{:S(2)}) collective-permute-start(bf16[256,128]{1,0:T(8,128)(2,1)} %get-tuple-element.13.own), channel_id=1, source_target_pairs={{0,8},{8,0},{1,9},{9,1},{2,10},{10,2},{3,11},{11,3},{4,12},{12,4},... | collective-permute-start | bytes 196616 | tf_op jit(solution)/shard_map/ppermute | solution.py:158
  78.7 0.6 copy-start.12
  81.8 27.1 %all-to-all-start.1 = ((bf16[16,16,1024]{2,1,0:T(8,128)(2,1)}), bf16[16,16,1024]{2,1,0:T(8,128)(2,1)S(1)}, u32[]{:S(2)}, u32[]{:S(2)}) async-start(bf16[16,16,1024]{2,1,0:T(8,128)(2,1)} %bitcast.55), calls=%async_computation.1 | async-start | bytes 1048576 | tf_op jit(solution)/shard_map/all_to_all | solution.py:159
  109.8 10.9 %all-to-all-start.3 = ((bf16[8,256,128]{2,1,0:T(8,128)(2,1)}), bf16[8,256,128]{2,1,0:T(8,128)(2,1)S(1)}, u32[]{:S(2)}, u32[]{:S(2)}) async-start(bf16[8,256,128]{2,1,0:T(8,128)(2,1)} %bitcast.16), calls=%async_computation.3 | async-start | bytes 1048576 | tf_op jit(solution)/shard_map/all_to_all | solution.py:43
  120.7 6.3 %copy-start.5 = (bf16[8,256,128]{2,1,0:T(8,128)(2,1)}, bf16[8,256,128]{2,1,0:T(8,128)(2,1)S(1)}, u32[]{:S(2)}) copy-start(bf16[8,256,128]{2,1,0:T(8,128)(2,1)S(1)} %all-to-all-done.3.own) | copy-start | bytes 1572868
  121.9 32.8 %all-to-all-start.2 = ((bf16[32,16,1024]{2,1,0:T(8,128)(2,1)}), bf16[32,16,1024]{2,1,0:T(8,128)(2,1)S(1)}, u32[]{:S(2)}, u32[]{:S(2)}) async-start(bf16[32,16,1024]{2,1,0:T(8,128)(2,1)} %broadcast_in_dim.16), calls=%async_computation.2 | async-start | bytes 2097152 | tf_op jit(solution)/shard_map/all_to_all | solution.py:162
  127.0 3.8 %collective-permute-start.7 = (bf16[8,256,128]{2,1,0:T(8,128)(2,1)S(1)}, bf16[8,256,128]{2,1,0:T(8,128)(2,1)S(1)}, u32[]{:S(2)}, u32[]{:S(2)}) collective-permute-start(bf16[8,256,128]{2,1,0:T(8,128)(2,1)S(1)} %all-to-all-done.3.own), channel_id=1, source_target_pairs={{0,1},{1,0},{2,3},{3,2},{4,5},{5,4},{6,7},{7,6},{8,9},{9,8},{10,11... | collective-permute-start | bytes 1572872 | tf_op jit(solution)/shard_map/ppermute | solution.py:144
  130.9 23.8 %copy-start.11 = (bf16[8,256,128]{2,1,0:T(8,128)(2,1)}, bf16[8,256,128]{2,1,0:T(8,128)(2,1)S(1)}, u32[]{:S(2)}) copy-start(bf16[8,256,128]{2,1,0:T(8,128)(2,1)S(1)} %collective-permute-done.7.other) | copy-start | bytes 1572868
  154.7 1.0 copy-start.3
  158.9 6.4 %collective-permute-start.9 = (bf16[256,128]{1,0:T(8,128)(2,1)}, bf16[256,128]{1,0:T(8,128)(2,1)S(1)}, u32[]{:S(2)}, u32[]{:S(2)}) collective-permute-start(bf16[256,128]{1,0:T(8,128)(2,1)} %get-tuple-element.19.own), channel_id=1, source_target_pairs={{0,8},{8,0},{1,9},{9,1},{2,10},{10,2},{3,11},{11,3},{4,12},{12,4},... | collective-permute-start | bytes 196616 | tf_op jit(solution)/shard_map/ppermute | solution.py:158
  165.2 0.6 copy-start.13
  192.9 4.1 %copy-start.4 = (bf16[2,128,1024]{2,1,0:T(8,128)(2,1)S(1)}, bf16[2,128,1024]{2,1,0:T(8,128)(2,1)}, u32[]{:S(2)}) copy-start(bf16[2,128,1024]{2,1,0:T(8,128)(2,1)} %get-tuple-element.15.send) | copy-start | bytes 1572868
  192.9 40.0 %copy-start.1 = (bf16[2,128,1024]{2,1,0:T(8,128)(2,1)S(1)}, bf16[2,128,1024]{2,1,0:T(8,128)(2,1)}, u32[]{:S(2)}) copy-start(bf16[2,128,1024]{2,1,0:T(8,128)(2,1)} %get-tuple-element.14.keep) | copy-start | bytes 1572868
  192.9 44.3 %all-to-all-start.5 = ((bf16[32,16,1024]{2,1,0:T(8,128)(2,1)}), bf16[32,16,1024]{2,1,0:T(8,128)(2,1)S(1)}, u32[]{:S(2)}, u32[]{:S(2)}) async-start(bf16[32,16,1024]{2,1,0:T(8,128)(2,1)} %broadcast_in_dim.37), calls=%async_computation.5 | async-start | bytes 2097152 | tf_op jit(solution)/shard_map/all_to_all | solution.py:162
  197.0 35.8 %collective-permute-start.8 = (bf16[2,128,1024]{2,1,0:T(8,128)(2,1)S(1)}, bf16[2,128,1024]{2,1,0:T(8,128)(2,1)S(1)}, u32[]{:S(2)}, u32[]{:S(2)}) collective-permute-start(bf16[2,128,1024]{2,1,0:T(8,128)(2,1)S(1)} %copy-done.4), channel_id=1, source_target_pairs={{0,8},{8,0},{1,9},{9,1},{2,10},{10,2},{3,11},{11,3},{4,12},{12,4},... | collective-permute-start | bytes 1572872 | tf_op jit(solution)/shard_map/ppermute | solution.py:146
  232.9 1.1 copy-start.8
  233.0 1.6 copy-start.10
  234.5 1.2 copy-start.7
  234.5 1.6 copy-start.9

commit v3 on v2

--- a/solution.py
+++ b/solution.py
@@ -5,6 +5,7 @@
 from jax.experimental.pallas import tpu as pltpu
 from jax.sharding import Mesh
 from jax.sharding import PartitionSpec as P
+
 
 norm_eps = 1e-06
 bf16 = jnp.bfloat16
@@ -31,6 +32,26 @@
         to = device(((fs >> 1) & 1) ^ k, 2 * (8 * gr + tp) + (fs & 1), fs >> 2)
         moves.append((device(gr, fs, tp), to))
     return moves
+
+
+def in_vmem(value):
+    return pltpu.with_memory_space_constraint(value, pltpu.VMEM)
+
+
+def kernel(body, outs, scratch=()):
+    here = pl.BlockSpec(memory_space=pltpu.VMEM)
+
+    def call(*args):
+        return pl.pallas_call(
+            body,
+            in_specs=[here] * len(args),
+            out_specs=tuple(here for _ in outs),
+            out_shape=tuple(pltpu.VMEM(shape, bf16) for shape in outs),
+            scratch_shapes=[pltpu.VMEM(shape, bf16) for shape in scratch],
+            compiler_params=pltpu.CompilerParams(vmem_limit_bytes=16 << 20),
+        )(*[in_vmem(a) for a in args])
+
+    return call
 
 
 def in_order(first, second, swapped):
@@ -83,16 +104,8 @@
         gate_act, up_act = act[:, :128], act[:, 128:]
         hidden[...] = (gate_act / (1.0 + jnp.exp(-gate_act)) * up_act).astype(bf16)
 
-    return pl.pallas_call(
-        body,
-        out_shape=(
-            jax.ShapeDtypeStruct((2048, 128), bf16),
-            jax.ShapeDtypeStruct((2048, 128), bf16),
-            jax.ShapeDtypeStruct((256, 128), bf16),
-        ),
-        scratch_shapes=[pltpu.VMEM((2048, 256), bf16)],
-        name="late_up" if late else "early_up",
-    )(stream, own, other)
+    outs = ((2048, 128), (2048, 128), (256, 128))
+    return kernel(body, outs, ((2048, 256),))(stream, own, other)
 
 
 def down_rows_call(own, other):
@@ -111,8 +124,7 @@
                     keep[k, :, col : col + 128] = jnp.where(even, line[0], line[1])
                     send[k, :, col : col + 128] = jnp.where(even, line[1], line[0])
 
-    shape = jax.ShapeDtypeStruct((2, 128, 1024), bf16)
-    return pl.pallas_call(body, out_shape=(shape, shape), name="down_rows")(own, other)
+    return kernel(body, ((2, 128, 1024), (2, 128, 1024)))(own, other)
 
 
 def down_call(layer, own, other, keep, send):
@@ -121,27 +133,28 @@
         act = act + jnp.dot(other[...], send[layer], preferred_element_type=f32)
         out[...] = act.astype(bf16)
 
-    return pl.pallas_call(
-        body, out_shape=jax.ShapeDtypeStruct((256, 1024), bf16), name="down"
-    )(own, other, keep, send)
+    return kernel(body, ((256, 1024),))(own, other, keep, send)[0]
 
 
-def per_device(prompt, norm_gain, gate_weight, up_weight, down_weight):
+def step(prompt, norm_gain, gate_weight, up_weight, down_weight):
     gain = norm_gain[:, :, None]
     gate = (gain * gate_weight).astype(bf16)
     up = (gain * up_weight).astype(bf16)
     high = lax.axis_index("gr") == 1
-    rows = []
+    moved = []
     for layer in range(2):
         block = jnp.concatenate([gate[layer], up[layer]], axis=0)
-        got = [lax.ppermute(block, AXES, weight_moves(k)) for k in range(2)]
-        rows.append(in_order(*got, high))
+        moved.append([lax.ppermute(block, AXES, weight_moves(k)) for k in range(2)])
     down = down_weight.astype(bf16).reshape(256, 128)
-    downs = in_order(down, lax.ppermute(down, "gr", SWAP), high)
-    early = halves_to_all([jnp.concatenate([*columns(rows[0], b), downs[b]]) for b in range(2)])
-    early = early, lax.ppermute(early, "core", SWAP)
-    late = halves_to_all([jnp.concatenate(columns(rows[1], b)) for b in range(2)])
-    late = late, lax.ppermute(late, "core", SWAP)
+    across = lax.ppermute(down, "gr", SWAP)
+    downs = in_order(down, across, high)
+    rows = in_order(*moved[0], high)
+    own = halves_to_all([jnp.concatenate([*columns(rows, b), downs[b]]) for b in range(2)])
+    own, *late = lax.optimization_barrier((own, *moved[1]))
+    rows = in_order(*late, high)
+    early = own, lax.ppermute(own, "core", SWAP)
+    own = halves_to_all([jnp.concatenate(columns(rows, b)) for b in range(2)])
+    late = own, lax.ppermute(own, "core", SWAP)
     keep, send = down_rows_call(*early)
     came = lax.ppermute(send, "yl", SWAP)
 
@@ -155,11 +168,13 @@
         gate, up, hidden = up_call(layer == 1, stream, *(late if layer else early))
         gates.append(gate)
         ups.append(up)
-        part = down_call(layer, hidden, lax.ppermute(hidden, "yl", SWAP), keep, send)
+        other = lax.ppermute(hidden, "yl", SWAP)
+        part = down_call(layer, hidden, other, keep, send)
         parts = lax.all_to_all(part.reshape(16, 16, 1024), ("zl", "yh"), 0, 0, tiled=True)
         mine = mine + 0.5 * jnp.sum(parts.astype(f32), axis=0)
         sends = jnp.broadcast_to(mine.astype(bf16)[None], (32, 16, 1024))
-        stream = lax.all_to_all(sends, ("yl", "zl", "yh"), 0, 0, tiled=True).reshape(2, 256, 1024)
+        stream = lax.all_to_all(sends, ("yl", "zl", "yh"), 0, 0, tiled=True)
+        stream = stream.reshape(2, 256, 1024)
     mixed = jnp.concatenate(list(stream), axis=1)
     served = jnp.concatenate(in_order(keep, came, yl == 1), axis=2)
     return jnp.stack(gates), jnp.stack(ups), served, mixed[None]
@@ -169,6 +184,4 @@
     fine = Mesh(mesh.devices.reshape(SIZES), AXES)
     in_specs = (P(GT, None, None), P(None, FS), P(None, FS, GT), P(None, FS, GT), P(None, FS, GT))
     out_specs = (P(None, None, FS), P(None, None, FS), P(None, FS, None), P(GT, None, None))
-    return jax.shard_map(
-        per_device, mesh=fine, in_specs=in_specs, out_specs=out_specs, check_vma=False
-    )
+    return jax.shard_map(step, mesh=fine, in_specs=in_specs, out_specs=out_specs, check_vma=False)

time: 240 us -> 225 us (0.938)
  the two profiles are of different devices: /device:TPU:2 before, /device:TPU:1 now
where the time goes in v3:
time: 225 us; the launch traced here: 223 us
  waiting for transfers between devices  94.1 us (42%)
  starting transfers between devices  86.7 us (39%)
  blocking collectives  22.8 us (10%)
  other arithmetic  8.18 us (4%)
  local copies, waits for them, and re-layouts  6.75 us (3%)
  Pallas kernels  3.87 us (2%)
    ppermute x1, waiting for transfers between devices, step(): came = lax.ppermute(send, 'yl', SWAP)  32.1 us
    ppermute x4, starting transfers between devices, step(): moved.append([lax.ppermute(block, AXES, weight_moves(k)) for k in range(2)])  29.4 us
    all_to_all x1, blocking collectives, step(): lax.all_to_all(part.reshape(16, 16, 1024), ('zl', 'yh'), 0, 0, tiled=True)  22.8 us
    all_to_all x2, waiting for transfers between devices, step(): stream = lax.all_to_all(sends, ('yl', 'zl', 'yh'), 0, 0, tiled=True)  18.2 us
    all_to_all x1, waiting for transfers between devices, step(): lax.all_to_all(part.reshape(16, 16, 1024), ('zl', 'yh'), 0, 0, tiled=True)  16.9 us
    all_to_all x2, starting transfers between devices, step(): stream = lax.all_to_all(sends, ('yl', 'zl', 'yh'), 0, 0, tiled=True)  12.7 us
    all_to_all x2, starting transfers between devices, halves_to_all(): return lax.all_to_all(sends, ('x', 'yl'), 0, 0, tiled=True)  11 us
    ppermute x2, starting transfers between devices, step(): other = lax.ppermute(hidden, 'yl', SWAP)  10.5 us
  transfers between devices with their start and end apart: 15, of which 11 were waited for; matrix products, arithmetic and copies ran while one was open for 2% of the time, Pallas kernels for 0%

profile of v3, /device:TPU:1, one launch (start us, length us, event | category | flops | bytes accessed | tf_op | source)
XLA Modules:
  0.0 223.4 jit_solution(16080421599508226071)
XLA Ops:
  0.6 1.1 multiply_convert_fusion.1
  1.8 14.0 %collective-permute-start = (bf16[128,256]{1,0:T(8,128)(2,1)S(1)}, bf16[128,256]{1,0:T(8,128)(2,1)S(1)}, u32[]{:S(2)}, u32[]{:S(2)}) collective-permute-start(bf16[128,256]{1,0:T(8,128)(2,1)S(1)} %pad_maximum_fusion.5), channel_id=1, source_target_pairs={{0,256},{1,272},{2,288},{3,304},{4,320},{5,336},{6,352},{7,368},{8... | collective-permute-start | bytes 196616 | tf_op jit(solution)/shard_map/ppermute | solution.py:147
  15.8 1.9 collective-permute-start.1
  18.7 4.0 %collective-permute-start.2 = (bf16[256,128]{1,0:T(8,128)(2,1)S(1)}, bf16[256,128]{1,0:T(8,128)(2,1)S(1)}, u32[]{:S(2)}, u32[]{:S(2)}) collective-permute-start(bf16[256,128]{1,0:T(8,128)(2,1)S(1)} %bitcast.62), channel_id=1, source_target_pairs={{0,256},{256,0},{1,257},{257,1},{2,258},{258,2},{3,259},{259,3},{4... | collective-permute-start | bytes 196616 | tf_op jit(solution)/shard_map/ppermute | solution.py:149
  22.7 2.7 %collective-permute-done.1 = bf16[128,256]{1,0:T(8,128)(2,1)S(1)} collective-permute-done((bf16[128,256]{1,0:T(8,128)(2,1)S(1)}, bf16[128,256]{1,0:T(8,128)(2,1)S(1)}, u32[]{:S(2)}, u32[]{:S(2)}) %collective-permute-start.1) | collective-permute-done | bytes 65568 | tf_op jit(solution)/shard_map/ppermute | solution.py:147
  25.5 4.1 %collective-permute-done.2 = bf16[256,128]{1,0:T(8,128)(2,1)S(1)} collective-permute-done((bf16[256,128]{1,0:T(8,128)(2,1)S(1)}, bf16[256,128]{1,0:T(8,128)(2,1)S(1)}, u32[]{:S(2)}, u32[]{:S(2)}) %collective-permute-start.2) | collective-permute-done | bytes 65568 | tf_op jit(solution)/shard_map/ppermute | solution.py:149
  29.7 1.1 broadcast_in_dim.14
  30.8 6.8 %all-to-all-start = ((bf16[8,512,128]{2,1,0:T(8,128)(2,1)}), bf16[8,512,128]{2,1,0:T(8,128)(2,1)S(1)}, u32[]{:S(2)}, u32[]{:S(2)}) async-start(bf16[8,512,128]{2,1,0:T(8,128)(2,1)} %bitcast.6), calls=%async_computation | async-start | bytes 2097152 | tf_op jit(solution)/shard_map/all_to_all | solution.py:64
  37.6 5.3 %collective-permute-start.3 = (bf16[128,256]{1,0:T(8,128)(2,1)S(1)}, bf16[128,256]{1,0:T(8,128)(2,1)S(1)}, u32[]{:S(2)}, u32[]{:S(2)}) collective-permute-start(bf16[128,256]{1,0:T(8,128)(2,1)S(1)} %pad_maximum_fusion.6), channel_id=1, source_target_pairs={{0,0},{1,16},{2,32},{3,48},{4,64},{5,80},{6,96},{7,112},{8,8},{9,2... | collective-permute-start | bytes 196616 | tf_op jit(solution)/shard_map/ppermute | solution.py:147
  42.9 8.2 %collective-permute-start.4 = (bf16[128,256]{1,0:T(8,128)(2,1)S(1)}, bf16[128,256]{1,0:T(8,128)(2,1)S(1)}, u32[]{:S(2)}, u32[]{:S(2)}) collective-permute-start(bf16[128,256]{1,0:T(8,128)(2,1)S(1)} %pad_maximum_fusion.6), channel_id=1, source_target_pairs={{0,256},{1,272},{2,288},{3,304},{4,320},{5,336},{6,352},{7,368},{8... | collective-permute-start | bytes 196616 | tf_op jit(solution)/shard_map/ppermute | solution.py:147
  51.1 5.5 %collective-permute-done.3 = bf16[128,256]{1,0:T(8,128)(2,1)S(1)} collective-permute-done((bf16[128,256]{1,0:T(8,128)(2,1)S(1)}, bf16[128,256]{1,0:T(8,128)(2,1)S(1)}, u32[]{:S(2)}, u32[]{:S(2)}) %collective-permute-start.3) | collective-permute-done | bytes 65568 | tf_op jit(solution)/shard_map/ppermute | solution.py:147
  56.6 1.9 collective-permute-start.5
  58.5 2.6 %collective-permute-done.5.other = bf16[8,512,128]{2,1,0:T(8,128)(2,1)S(1)} collective-permute-done((bf16[8,512,128]{2,1,0:T(8,128)(2,1)S(1)}, bf16[8,512,128]{2,1,0:T(8,128)(2,1)S(1)}, u32[]{:S(2)}, u32[]{:S(2)}) %collective-permute-start.5) | collective-permute-done | bytes 1048608 | tf_op jit(solution)/shard_map/ppermute | solution.py:155
  62.1 6.1 %collective-permute-start.6 = (bf16[256,128]{1,0:T(8,128)(2,1)S(1)}, bf16[256,128]{1,0:T(8,128)(2,1)S(1)}, u32[]{:S(2)}, u32[]{:S(2)}) collective-permute-start(bf16[256,128]{1,0:T(8,128)(2,1)S(1)} %get-tuple-element.17.own), channel_id=1, source_target_pairs={{0,8},{8,0},{1,9},{9,1},{2,10},{10,2},{3,11},{11,3},{4,12},{12,4},... | collective-permute-start | bytes 196616 | tf_op jit(solution)/shard_map/ppermute | solution.py:171
  68.6 2.0 collective-permute-done.6.other
  70.6 1.2 shard_map.86
  71.8 10.2 %all-to-all-start.1 = ((bf16[16,16,1024]{2,1,0:T(8,128)(2,1)}), bf16[16,16,1024]{2,1,0:T(8,128)(2,1)S(1)}, u32[]{:S(2)}, u32[]{:S(2)}) async-start(bf16[16,16,1024]{2,1,0:T(8,128)(2,1)} %bitcast.10), calls=%async_computation.1 | async-start | bytes 1048576 | tf_op jit(solution)/shard_map/all_to_all | solution.py:173
  82.1 16.9 %all-to-all-done.1 = bf16[16,16,1024]{2,1,0:T(8,128)(2,1)S(1)} async-done(((bf16[16,16,1024]{2,1,0:T(8,128)(2,1)}), bf16[16,16,1024]{2,1,0:T(8,128)(2,1)S(1)}, u32[]{:S(2)}, u32[]{:S(2)}) %all-to-all-start.1) | async-done | bytes 524320 | tf_op jit(solution)/shard_map/all_to_all | solution.py:173
  99.8 4.2 %all-to-all-start.3 = ((bf16[8,256,128]{2,1,0:T(8,128)(2,1)}), bf16[8,256,128]{2,1,0:T(8,128)(2,1)S(1)}, u32[]{:S(2)}, u32[]{:S(2)}) async-start(bf16[8,256,128]{2,1,0:T(8,128)(2,1)} %bitcast.16), calls=%async_computation.3 | async-start | bytes 1048576 | tf_op jit(solution)/shard_map/all_to_all | solution.py:64
  104.9 6.8 %all-to-all-done.3.own = bf16[8,256,128]{2,1,0:T(8,128)(2,1)S(1)} async-done(((bf16[8,256,128]{2,1,0:T(8,128)(2,1)}), bf16[8,256,128]{2,1,0:T(8,128)(2,1)S(1)}, u32[]{:S(2)}, u32[]{:S(2)}) %all-to-all-start.3) | async-done | bytes 524320 | tf_op jit(solution)/shard_map/all_to_all | solution.py:64
  111.6 1.1 broadcast_in_dim.16
  112.7 6.4 %all-to-all-start.2 = ((bf16[32,16,1024]{2,1,0:T(8,128)(2,1)}), bf16[32,16,1024]{2,1,0:T(8,128)(2,1)S(1)}, u32[]{:S(2)}, u32[]{:S(2)}) async-start(bf16[32,16,1024]{2,1,0:T(8,128)(2,1)} %broadcast_in_dim.16), calls=%async_computation.2 | async-start | bytes 2097152 | tf_op jit(solution)/shard_map/all_to_all | solution.py:176
  119.2 3.9 %collective-permute-start.7 = (bf16[8,256,128]{2,1,0:T(8,128)(2,1)S(1)}, bf16[8,256,128]{2,1,0:T(8,128)(2,1)S(1)}, u32[]{:S(2)}, u32[]{:S(2)}) collective-permute-start(bf16[8,256,128]{2,1,0:T(8,128)(2,1)S(1)} %all-to-all-done.3.own), channel_id=1, source_target_pairs={{0,1},{1,0},{2,3},{3,2},{4,5},{5,4},{6,7},{7,6},{8,9},{9,8},{10,11... | collective-permute-start | bytes 1572872 | tf_op jit(solution)/shard_map/ppermute | solution.py:157
  123.1 1.5 collective-permute-done.7.other
  125.4 18.2 %all-to-all-done.2 = bf16[32,16,1024]{2,1,0:T(8,128)(2,1)S(1)} async-done(((bf16[32,16,1024]{2,1,0:T(8,128)(2,1)}), bf16[32,16,1024]{2,1,0:T(8,128)(2,1)S(1)}, u32[]{:S(2)}, u32[]{:S(2)}) %all-to-all-start.2) | async-done | bytes 1048608 | tf_op jit(solution)/shard_map/all_to_all | solution.py:176
  145.6 4.4 %collective-permute-start.9 = (bf16[256,128]{1,0:T(8,128)(2,1)S(1)}, bf16[256,128]{1,0:T(8,128)(2,1)S(1)}, u32[]{:S(2)}, u32[]{:S(2)}) collective-permute-start(bf16[256,128]{1,0:T(8,128)(2,1)S(1)} %get-tuple-element.25.own), channel_id=1, source_target_pairs={{0,8},{8,0},{1,9},{9,1},{2,10},{10,2},{3,11},{11,3},{4,12},{12,4},... | collective-permute-start | bytes 196616 | tf_op jit(solution)/shard_map/ppermute | solution.py:171
  150.0 1.6 collective-permute-done.9.other
  152.1 22.8 %all_to_all.30 = bf16[16,16,1024]{2,1,0:T(8,128)(2,1)S(1)} all-to-all(bf16[16,16,1024]{2,1,0:T(8,128)(2,1)S(1)} %bitcast.54), channel_id=1, replica_groups=mesh['gr'=2,'zl'=4,'yh'=4,'yl'=2,'x'=4,'core'=2] {'zl','yh'}, dimensions={0} | all-to-all | bytes 1048576 | tf_op jit(solution)/shard_map/all_to_all | solution.py:173
  175.7 1.1 broadcast_in_dim.37
  176.8 6.3 %all-to-all-start.5 = ((bf16[32,16,1024]{2,1,0:T(8,128)(2,1)}), bf16[32,16,1024]{2,1,0:T(8,128)(2,1)S(1)}, u32[]{:S(2)}, u32[]{:S(2)}) async-start(bf16[32,16,1024]{2,1,0:T(8,128)(2,1)} %broadcast_in_dim.37), calls=%async_computation.5 | async-start | bytes 2097152 | tf_op jit(solution)/shard_map/all_to_all | solution.py:176
  183.1 3.1 %collective-permute-start.8 = (bf16[2,128,1024]{2,1,0:T(8,128)(2,1)S(1)}, bf16[2,128,1024]{2,1,0:T(8,128)(2,1)S(1)}, u32[]{:S(2)}, u32[]{:S(2)}) collective-permute-start(bf16[2,128,1024]{2,1,0:T(8,128)(2,1)S(1)} %get-tuple-element.19.send), channel_id=1, source_target_pairs={{0,8},{8,0},{1,9},{9,1},{2,10},{10,2},{3,11},{11,3},{4,12},{12,4},... | collective-permute-start | bytes 1572872 | tf_op jit(solution)/shard_map/ppermute | solution.py:159
  186.2 32.1 %collective-permute-done.8 = bf16[2,128,1024]{2,1,0:T(8,128)(2,1)S(1)} collective-permute-done((bf16[2,128,1024]{2,1,0:T(8,128)(2,1)S(1)}, bf16[2,128,1024]{2,1,0:T(8,128)(2,1)S(1)}, u32[]{:S(2)}, u32[]{:S(2)}) %collective-permute-start.8) | collective-permute-done | bytes 524320 | tf_op jit(solution)/shard_map/ppermute | solution.py:159
  (56 shorter events, 13.2 us)
Async XLA Ops:
  0.6 29.0 %copy-start.9 = (f32[2,128,128]{2,1,0:T(8,128)S(1)}, f32[2,128,128]{2,1,0:T(8,128)}, u32[]{:S(2)}) copy-start(f32[2,128,128]{2,1,0:T(8,128)} %param.9) | copy-start | bytes 393220
  1.8 20.9 %collective-permute-start = (bf16[128,256]{1,0:T(8,128)(2,1)S(1)}, bf16[128,256]{1,0:T(8,128)(2,1)S(1)}, u32[]{:S(2)}, u32[]{:S(2)}) collective-permute-start(bf16[128,256]{1,0:T(8,128)(2,1)S(1)} %pad_maximum_fusion.5), channel_id=1, source_target_pairs={{0,256},{1,272},{2,288},{3,304},{4,320},{5,336},{6,352},{7,368},{8... | collective-permute-start | bytes 196616 | tf_op jit(solution)/shard_map/ppermute | solution.py:147
  15.8 9.6 %collective-permute-start.1 = (bf16[128,256]{1,0:T(8,128)(2,1)S(1)}, bf16[128,256]{1,0:T(8,128)(2,1)S(1)}, u32[]{:S(2)}, u32[]{:S(2)}) collective-permute-start(bf16[128,256]{1,0:T(8,128)(2,1)S(1)} %pad_maximum_fusion.5), channel_id=1, source_target_pairs={{0,0},{1,16},{2,32},{3,48},{4,64},{5,80},{6,96},{7,112},{8,8},{9,2... | collective-permute-start | bytes 196616 | tf_op jit(solution)/shard_map/ppermute | solution.py:147
  18.7 10.9 %collective-permute-start.2 = (bf16[256,128]{1,0:T(8,128)(2,1)S(1)}, bf16[256,128]{1,0:T(8,128)(2,1)S(1)}, u32[]{:S(2)}, u32[]{:S(2)}) collective-permute-start(bf16[256,128]{1,0:T(8,128)(2,1)S(1)} %bitcast.62), channel_id=1, source_target_pairs={{0,256},{256,0},{1,257},{257,1},{2,258},{258,2},{3,259},{259,3},{4... | collective-permute-start | bytes 196616 | tf_op jit(solution)/shard_map/ppermute | solution.py:149
  30.8 30.4 %copy-start = (bf16[1,256,2048]{2,1,0:T(8,128)(2,1)S(1)}, bf16[1,256,2048]{2,1,0:T(8,128)(2,1)}, u32[]{:S(2)}) copy-start(bf16[1,256,2048]{2,1,0:T(8,128)(2,1)} %param.5) | copy-start | bytes 3145732
  30.8 25.8 %all-to-all-start = ((bf16[8,512,128]{2,1,0:T(8,128)(2,1)}), bf16[8,512,128]{2,1,0:T(8,128)(2,1)S(1)}, u32[]{:S(2)}, u32[]{:S(2)}) async-start(bf16[8,512,128]{2,1,0:T(8,128)(2,1)} %bitcast.6), calls=%async_computation | async-start | bytes 2097152 | tf_op jit(solution)/shard_map/all_to_all | solution.py:64
  37.6 19.0 %collective-permute-start.3 = (bf16[128,256]{1,0:T(8,128)(2,1)S(1)}, bf16[128,256]{1,0:T(8,128)(2,1)S(1)}, u32[]{:S(2)}, u32[]{:S(2)}) collective-permute-start(bf16[128,256]{1,0:T(8,128)(2,1)S(1)} %pad_maximum_fusion.6), channel_id=1, source_target_pairs={{0,0},{1,16},{2,32},{3,48},{4,64},{5,80},{6,96},{7,112},{8,8},{9,2... | collective-permute-start | bytes 196616 | tf_op jit(solution)/shard_map/ppermute | solution.py:147
  42.9 13.7 %collective-permute-start.4 = (bf16[128,256]{1,0:T(8,128)(2,1)S(1)}, bf16[128,256]{1,0:T(8,128)(2,1)S(1)}, u32[]{:S(2)}, u32[]{:S(2)}) collective-permute-start(bf16[128,256]{1,0:T(8,128)(2,1)S(1)} %pad_maximum_fusion.6), channel_id=1, source_target_pairs={{0,256},{1,272},{2,288},{3,304},{4,320},{5,336},{6,352},{7,368},{8... | collective-permute-start | bytes 196616 | tf_op jit(solution)/shard_map/ppermute | solution.py:147
  56.6 4.5 %collective-permute-start.5 = (bf16[8,512,128]{2,1,0:T(8,128)(2,1)S(1)}, bf16[8,512,128]{2,1,0:T(8,128)(2,1)S(1)}, u32[]{:S(2)}, u32[]{:S(2)}) collective-permute-start(bf16[8,512,128]{2,1,0:T(8,128)(2,1)S(1)} %all-to-all-done.own), channel_id=1, source_target_pairs={{0,1},{1,0},{2,3},{3,2},{4,5},{5,4},{6,7},{7,6},{8,9},{9,8},{10,11... | collective-permute-start | bytes 3145736 | tf_op jit(solution)/shard_map/ppermute | solution.py:155
  62.1 6.5 %copy-start.1 = (bf16[2048,128]{1,0:T(8,128)(2,1)}, bf16[2048,128]{1,0:T(8,128)(2,1)S(1)}, u32[]{:S(2)}) copy-start(bf16[2048,128]{1,0:T(8,128)(2,1)S(1)} %get-tuple-element.23) | copy-start | bytes 1572868
  62.1 8.4 %collective-permute-start.6 = (bf16[256,128]{1,0:T(8,128)(2,1)S(1)}, bf16[256,128]{1,0:T(8,128)(2,1)S(1)}, u32[]{:S(2)}, u32[]{:S(2)}) collective-permute-start(bf16[256,128]{1,0:T(8,128)(2,1)S(1)} %get-tuple-element.17.own), channel_id=1, source_target_pairs={{0,8},{8,0},{1,9},{9,1},{2,10},{10,2},{3,11},{11,3},{4,12},{12,4},... | collective-permute-start | bytes 196616 | tf_op jit(solution)/shard_map/ppermute | solution.py:171
  71.8 27.2 %all-to-all-start.1 = ((bf16[16,16,1024]{2,1,0:T(8,128)(2,1)}), bf16[16,16,1024]{2,1,0:T(8,128)(2,1)S(1)}, u32[]{:S(2)}, u32[]{:S(2)}) async-start(bf16[16,16,1024]{2,1,0:T(8,128)(2,1)} %bitcast.10), calls=%async_computation.1 | async-start | bytes 1048576 | tf_op jit(solution)/shard_map/all_to_all | solution.py:173
  99.8 11.8 %all-to-all-start.3 = ((bf16[8,256,128]{2,1,0:T(8,128)(2,1)}), bf16[8,256,128]{2,1,0:T(8,128)(2,1)S(1)}, u32[]{:S(2)}, u32[]{:S(2)}) async-start(bf16[8,256,128]{2,1,0:T(8,128)(2,1)} %bitcast.16), calls=%async_computation.3 | async-start | bytes 1048576 | tf_op jit(solution)/shard_map/all_to_all | solution.py:64
  112.7 30.9 %all-to-all-start.2 = ((bf16[32,16,1024]{2,1,0:T(8,128)(2,1)}), bf16[32,16,1024]{2,1,0:T(8,128)(2,1)S(1)}, u32[]{:S(2)}, u32[]{:S(2)}) async-start(bf16[32,16,1024]{2,1,0:T(8,128)(2,1)} %broadcast_in_dim.16), calls=%async_computation.2 | async-start | bytes 2097152 | tf_op jit(solution)/shard_map/all_to_all | solution.py:176
  119.2 5.5 %collective-permute-start.7 = (bf16[8,256,128]{2,1,0:T(8,128)(2,1)S(1)}, bf16[8,256,128]{2,1,0:T(8,128)(2,1)S(1)}, u32[]{:S(2)}, u32[]{:S(2)}) collective-permute-start(bf16[8,256,128]{2,1,0:T(8,128)(2,1)S(1)} %all-to-all-done.3.own), channel_id=1, source_target_pairs={{0,1},{1,0},{2,3},{3,2},{4,5},{5,4},{6,7},{7,6},{8,9},{9,8},{10,11... | collective-permute-start | bytes 1572872 | tf_op jit(solution)/shard_map/ppermute | solution.py:157
  124.6 0.8 copy-start.7
  143.6 1.0 copy-start.8
  145.6 29.2 %copy-start.3 = (bf16[2048,128]{1,0:T(8,128)(2,1)}, bf16[2048,128]{1,0:T(8,128)(2,1)S(1)}, u32[]{:S(2)}) copy-start(bf16[2048,128]{1,0:T(8,128)(2,1)S(1)} %get-tuple-element.22) | copy-start | bytes 1572868
  145.6 29.2 %copy-start.5 = (bf16[2048,128]{1,0:T(8,128)(2,1)}, bf16[2048,128]{1,0:T(8,128)(2,1)S(1)}, u32[]{:S(2)}) copy-start(bf16[2048,128]{1,0:T(8,128)(2,1)S(1)} %get-tuple-element.24) | copy-start | bytes 1572868
  145.6 6.0 %collective-permute-start.9 = (bf16[256,128]{1,0:T(8,128)(2,1)S(1)}, bf16[256,128]{1,0:T(8,128)(2,1)S(1)}, u32[]{:S(2)}, u32[]{:S(2)}) collective-permute-start(bf16[256,128]{1,0:T(8,128)(2,1)S(1)} %get-tuple-element.25.own), channel_id=1, source_target_pairs={{0,8},{8,0},{1,9},{9,1},{2,10},{10,2},{3,11},{11,3},{4,12},{12,4},... | collective-permute-start | bytes 196616 | tf_op jit(solution)/shard_map/ppermute | solution.py:171
  176.8 45.4 %all-to-all-start.5 = ((bf16[32,16,1024]{2,1,0:T(8,128)(2,1)}), bf16[32,16,1024]{2,1,0:T(8,128)(2,1)S(1)}, u32[]{:S(2)}, u32[]{:S(2)}) async-start(bf16[32,16,1024]{2,1,0:T(8,128)(2,1)} %broadcast_in_dim.37), calls=%async_computation.5 | async-start | bytes 2097152 | tf_op jit(solution)/shard_map/all_to_all | solution.py:176
  183.1 35.3 %collective-permute-start.8 = (bf16[2,128,1024]{2,1,0:T(8,128)(2,1)S(1)}, bf16[2,128,1024]{2,1,0:T(8,128)(2,1)S(1)}, u32[]{:S(2)}, u32[]{:S(2)}) collective-permute-start(bf16[2,128,1024]{2,1,0:T(8,128)(2,1)S(1)} %get-tuple-element.19.send), channel_id=1, source_target_pairs={{0,8},{8,0},{1,9},{9,1},{2,10},{10,2},{3,11},{11,3},{4,12},{12,4},... | collective-permute-start | bytes 1572872 | tf_op jit(solution)/shard_map/ppermute | solution.py:159
  218.5 1.1 copy-start.2
  218.5 1.6 copy-start.6
  220.0 1.2 copy-start.4

commit v4 on v3

--- a/solution.py
+++ b/solution.py
@@ -26,10 +26,10 @@
     return [(gr, fs, tp) for gr in range(2) for fs in range(32) for tp in range(8)]
 
 
-def weight_moves(k):
+def weight_moves():
     moves = []
     for gr, fs, tp in everyone():
-        to = device(((fs >> 1) & 1) ^ k, 2 * (8 * gr + tp) + (fs & 1), fs >> 2)
+        to = device(fs >> 4, 2 * (8 * gr + tp) + (fs & 1), (fs >> 1) & 7)
         moves.append((device(gr, fs, tp), to))
     return moves
 
@@ -77,35 +77,43 @@
                 ot = other[2 * x + b, 128 * s : 128 * s + 128]
                 for c in range(2):
                     line = jnp.where(mine, mn, ot) if c == 0 else jnp.where(mine, ot, mn)
-                    at = 64 * (8 * x + 4 * c + 2 * s + b)
+                    at = 64 * (16 * s + 4 * x + 2 * c + b)
                     both[at : at + 64, :128] = line[:64]
                     both[at : at + 64, 128:] = line[64:]
 
 
 def up_call(late, stream, own, other):
-    def part_of(stream, z):
-        if late:
-            return stream[z // 2, :, 512 * (z % 2) : 512 * (z % 2) + 512].astype(f32)
-        return stream[:, 512 * z : 512 * z + 512].astype(f32)
-
     def body(stream, own, other, gate, up, hidden, both):
         gather_rows(lax.axis_index("core"), own, other, both)
         gate[...] = both[:, :128]
         up[...] = both[:, 128:]
-        squares = jnp.zeros((256, 1), f32)
-        for z in range(4):
-            part = part_of(stream, z)
-            squares = squares + jnp.sum(part * part, axis=1, keepdims=True)
-        scale = lax.rsqrt(squares * (1.0 / 2048) + norm_eps)
-        act = jnp.zeros((256, 256), f32)
-        for z in range(4):
-            normed = (part_of(stream, z) * scale).astype(bf16)
-            act = act + jnp.dot(normed, both[512 * z : 512 * z + 512], preferred_element_type=f32)
+        if late:
+            squares = jnp.zeros((256, 1), f32)
+            for z in range(4):
+                part = stream[z // 2, :, 512 * (z % 2) : 512 * (z % 2) + 512].astype(f32)
+                squares = squares + jnp.sum(part * part, axis=1, keepdims=True)
+            scale = lax.rsqrt(squares * (1.0 / 2048) + norm_eps)
+            act = jnp.zeros((256, 256), f32)
+            for z in range(4):
+                part = stream[z // 2, :, 512 * (z % 2) : 512 * (z % 2) + 512].astype(f32)
+                part = (part * scale).astype(bf16)
+                act = act + jnp.dot(part, both[512 * z : 512 * z + 512], preferred_element_type=f32)
+        else:
+            act = jnp.dot(stream[...], both[...], preferred_element_type=f32)
         gate_act, up_act = act[:, :128], act[:, 128:]
         hidden[...] = (gate_act / (1.0 + jnp.exp(-gate_act)) * up_act).astype(bf16)
 
     outs = ((2048, 128), (2048, 128), (256, 128))
     return kernel(body, outs, ((2048, 256),))(stream, own, other)
+
+
+def norm_call(stream):
+    def body(stream, out):
+        value = stream[...].astype(f32)
+        mean = jnp.sum(value * value, axis=1, keepdims=True) * (1.0 / 2048)
+        out[...] = (value * lax.rsqrt(mean + norm_eps)).astype(bf16)
+
+    return kernel(body, ((256, 2048),))(stream)[0]
 
 
 def down_rows_call(own, other):
@@ -144,13 +152,19 @@
     moved = []
     for layer in range(2):
         block = jnp.concatenate([gate[layer], up[layer]], axis=0)
-        moved.append([lax.ppermute(block, AXES, weight_moves(k)) for k in range(2)])
-    down = down_weight.astype(bf16).reshape(256, 128)
-    across = lax.ppermute(down, "gr", SWAP)
-    downs = in_order(down, across, high)
-    rows = in_order(*moved[0], high)
-    own = halves_to_all([jnp.concatenate([*columns(rows, b), downs[b]]) for b in range(2)])
-    own, *late = lax.optimization_barrier((own, *moved[1]))
+        moved.append(lax.ppermute(block, AXES, weight_moves()))
+    down = down_weight.astype(bf16)
+    down = jnp.concatenate([down[0], down[1]], axis=1)
+    both = jnp.concatenate([moved[0], down], axis=0)
+    across = lax.ppermute(both, "gr", SWAP)
+    rows = in_order(both, across, high)
+    blocks = []
+    for b in range(2):
+        lower = [rows[b][128:, :128], rows[b][128:, 128:]]
+        blocks.append(jnp.concatenate([*columns([r[:128] for r in rows], b), *lower]))
+    own = halves_to_all(blocks)
+    across = lax.ppermute(moved[1], "gr", SWAP)
+    own, *late = lax.optimization_barrier((own, moved[1], across))
     rows = in_order(*late, high)
     early = own, lax.ppermute(own, "core", SWAP)
     own = halves_to_all([jnp.concatenate(columns(rows, b)) for b in range(2)])
@@ -158,10 +172,10 @@
     keep, send = down_rows_call(*early)
     came = lax.ppermute(send, "yl", SWAP)
 
-    stream = prompt[0]
+    stream = norm_call(prompt[0])
     yl = lax.axis_index("yl")
     mine = lax.dynamic_slice(
-        stream, (lax.axis_index(("zl", "yh")) * 16, yl * 1024), (16, 1024)
+        prompt[0], (lax.axis_index(("zl", "yh")) * 16, yl * 1024), (16, 1024)
     ).astype(f32)
     gates, ups = [], []
     for layer in range(2):

time: 225 us -> 235 us (1.044)
  starting transfers between devices: 86.7 us -> 96.2 us
    ppermute x2, starting transfers between devices: 10.5 us -> 14.7 us  [step(): other = lax.ppermute(hidden, 'yl', SWAP)]
    ppermute x1, starting transfers between devices: 1.91 us -> 5.62 us  [step(): early = (own, lax.ppermute(own, 'core', SWAP))]
    all_to_all x1, starting transfers between devices: 10.2 us -> 12.8 us  [step(): lax.all_to_all(part.reshape(16, 16, 1024), ('zl', 'yh'), 0, 0, tiled=True)]
    all_to_all x2, starting transfers between devices: 11 us -> 8.35 us  [halves_to_all(): return lax.all_to_all(sends, ('x', 'yl'), 0, 0, tiled=True)]
    ppermute x5 -> x4, starting transfers between devices: 33.4 us -> 36 us  [the longest x2 13.5 us: step(): moved.append(lax.ppermute(block, AXES, weight_moves()))]
    ppermute x5 -> x4, waiting for transfers between devices: 12.3 us -> 10.9 us  [the longest x1 6.18 us: step(): across = lax.ppermute(both, 'gr', SWAP)]
  transfers between devices with their start and end apart: 15 -> 14, of which waited for: 11 -> 12; matrix products, arithmetic and copies ran while one was open for 2% -> 2% of each run, Pallas kernels for 0% -> 0%
where the time goes in v4:
time: 235 us; the launch traced here: 233 us
  starting transfers between devices  96.2 us (41%)
  waiting for transfers between devices  94.7 us (40%)
  blocking collectives  22.7 us (10%)
  other arithmetic  8.18 us (3%)
  local copies, waits for them, and re-layouts  6.78 us (3%)
  Pallas kernels  3.93 us (2%)
    ppermute x1, waiting for transfers between devices, step(): came = lax.ppermute(send, 'yl', SWAP)  32.1 us
    all_to_all x1, blocking collectives, step(): lax.all_to_all(part.reshape(16, 16, 1024), ('zl', 'yh'), 0, 0, tiled=True)  22.7 us
    all_to_all x2, waiting for transfers between devices, step(): stream = lax.all_to_all(sends, ('yl', 'zl', 'yh'), 0, 0, tiled=True)  18.6 us
    all_to_all x1, waiting for transfers between devices, step(): lax.all_to_all(part.reshape(16, 16, 1024), ('zl', 'yh'), 0, 0, tiled=True)  18.5 us
    ppermute x2, starting transfers between devices, step(): other = lax.ppermute(hidden, 'yl', SWAP)  14.7 us
    ppermute x2, starting transfers between devices, step(): moved.append(lax.ppermute(block, AXES, weight_moves()))  13.5 us
    ppermute x1, starting transfers between devices, step(): across = lax.ppermute(both, 'gr', SWAP)  13.4 us
    all_to_all x1, starting transfers between devices, step(): lax.all_to_all(part.reshape(16, 16, 1024), ('zl', 'yh'), 0, 0, tiled=True)  12.8 us
  transfers between devices with their start and end apart: 14, of which 12 were waited for; matrix products, arithmetic and copies ran while one was open for 2% of the time, Pallas kernels for 0%

profile of v4, /device:TPU:1, one launch (start us, length us, event | category | flops | bytes accessed | tf_op | source)
XLA Modules:
  0.0 233.5 jit_solution(4089025508610855229)
XLA Ops:
  0.6 1.1 multiply_convert_fusion.1
  1.7 5.6 %collective-permute-start = (bf16[128,256]{1,0:T(8,128)(2,1)S(1)}, bf16[128,256]{1,0:T(8,128)(2,1)S(1)}, u32[]{:S(2)}, u32[]{:S(2)}) collective-permute-start(bf16[128,256]{1,0:T(8,128)(2,1)S(1)} %pad_maximum_fusion.5), channel_id=1, source_target_pairs={{0,0},{1,16},{2,32},{3,48},{4,64},{5,80},{6,96},{7,112},{8,8},{9,2... | collective-permute-start | bytes 196616 | tf_op jit(solution)/shard_map/ppermute | solution.py:155
  9.3 13.4 %collective-permute-start.1 = (bf16[256,256]{1,0:T(8,128)(2,1)S(1)}, bf16[256,256]{1,0:T(8,128)(2,1)S(1)}, u32[]{:S(2)}, u32[]{:S(2)}) collective-permute-start(bf16[256,256]{1,0:T(8,128)(2,1)S(1)} %maximum_maximum_fusion), channel_id=1, source_target_pairs={{0,256},{256,0},{1,257},{257,1},{2,258},{258,2},{3,259},{259,3},{4... | collective-permute-start | bytes 393224 | tf_op jit(solution)/shard_map/ppermute | solution.py:159
  22.8 6.2 %collective-permute-done.1 = bf16[256,256]{1,0:T(8,128)(2,1)S(1)} collective-permute-done((bf16[256,256]{1,0:T(8,128)(2,1)S(1)}, bf16[256,256]{1,0:T(8,128)(2,1)S(1)}, u32[]{:S(2)}, u32[]{:S(2)}) %collective-permute-start.1) | collective-permute-done | bytes 131104 | tf_op jit(solution)/shard_map/ppermute | solution.py:159
  29.1 1.1 broadcast_in_dim.14
  30.2 4.9 %all-to-all-start = ((bf16[8,512,128]{2,1,0:T(8,128)(2,1)}), bf16[8,512,128]{2,1,0:T(8,128)(2,1)S(1)}, u32[]{:S(2)}, u32[]{:S(2)}) async-start(bf16[8,512,128]{2,1,0:T(8,128)(2,1)} %bitcast.7), calls=%async_computation | async-start | bytes 2097152 | tf_op jit(solution)/shard_map/all_to_all | solution.py:64
  35.1 7.9 %collective-permute-start.2 = (bf16[128,256]{1,0:T(8,128)(2,1)S(1)}, bf16[128,256]{1,0:T(8,128)(2,1)S(1)}, u32[]{:S(2)}, u32[]{:S(2)}) collective-permute-start(bf16[128,256]{1,0:T(8,128)(2,1)S(1)} %pad_maximum_fusion.6), channel_id=1, source_target_pairs={{0,0},{1,16},{2,32},{3,48},{4,64},{5,80},{6,96},{7,112},{8,8},{9,2... | collective-permute-start | bytes 196616 | tf_op jit(solution)/shard_map/ppermute | solution.py:155
  43.0 2.0 collective-permute-done.2
  45.0 9.1 %collective-permute-start.3 = (bf16[128,256]{1,0:T(8,128)(2,1)S(1)}, bf16[128,256]{1,0:T(8,128)(2,1)S(1)}, u32[]{:S(2)}, u32[]{:S(2)}) collective-permute-start(bf16[128,256]{1,0:T(8,128)(2,1)S(1)} %collective-permute-done.2), channel_id=1, source_target_pairs={{0,256},{256,0},{1,257},{257,1},{2,258},{258,2},{3,259},{259,3},{4... | collective-permute-start | bytes 196616 | tf_op jit(solution)/shard_map/ppermute | solution.py:166
  54.1 1.6 collective-permute-done.3
  55.8 5.6 %collective-permute-start.4 = (bf16[8,512,128]{2,1,0:T(8,128)(2,1)S(1)}, bf16[8,512,128]{2,1,0:T(8,128)(2,1)S(1)}, u32[]{:S(2)}, u32[]{:S(2)}) collective-permute-start(bf16[8,512,128]{2,1,0:T(8,128)(2,1)S(1)} %all-to-all-done.own), channel_id=1, source_target_pairs={{0,1},{1,0},{2,3},{3,2},{4,5},{5,4},{6,7},{7,6},{8,9},{9,8},{10,11... | collective-permute-start | bytes 3145736 | tf_op jit(solution)/shard_map/ppermute | solution.py:169
  61.8 1.9 collective-permute-done.4.other
  64.4 10.5 %collective-permute-start.5 = (bf16[256,128]{1,0:T(8,128)(2,1)S(1)}, bf16[256,128]{1,0:T(8,128)(2,1)S(1)}, u32[]{:S(2)}, u32[]{:S(2)}) collective-permute-start(bf16[256,128]{1,0:T(8,128)(2,1)S(1)} %get-tuple-element.17.own), channel_id=1, source_target_pairs={{0,8},{8,0},{1,9},{9,1},{2,10},{10,2},{3,11},{11,3},{4,12},{12,4},... | collective-permute-start | bytes 196616 | tf_op jit(solution)/shard_map/ppermute | solution.py:185
  75.3 2.0 collective-permute-done.5.other
  77.2 1.2 shard_map.87
  78.4 12.8 %all-to-all-start.1 = ((bf16[16,16,1024]{2,1,0:T(8,128)(2,1)}), bf16[16,16,1024]{2,1,0:T(8,128)(2,1)S(1)}, u32[]{:S(2)}, u32[]{:S(2)}) async-start(bf16[16,16,1024]{2,1,0:T(8,128)(2,1)} %bitcast.11), calls=%async_computation.1 | async-start | bytes 1048576 | tf_op jit(solution)/shard_map/all_to_all | solution.py:187
  91.4 18.5 %all-to-all-done.1 = bf16[16,16,1024]{2,1,0:T(8,128)(2,1)S(1)} async-done(((bf16[16,16,1024]{2,1,0:T(8,128)(2,1)}), bf16[16,16,1024]{2,1,0:T(8,128)(2,1)S(1)}, u32[]{:S(2)}, u32[]{:S(2)}) %all-to-all-start.1) | async-done | bytes 524320 | tf_op jit(solution)/shard_map/all_to_all | solution.py:187
  110.7 3.5 %all-to-all-start.3 = ((bf16[8,256,128]{2,1,0:T(8,128)(2,1)}), bf16[8,256,128]{2,1,0:T(8,128)(2,1)S(1)}, u32[]{:S(2)}, u32[]{:S(2)}) async-start(bf16[8,256,128]{2,1,0:T(8,128)(2,1)} %bitcast.17), calls=%async_computation.3 | async-start | bytes 1048576 | tf_op jit(solution)/shard_map/all_to_all | solution.py:64
  115.1 7.6 %all-to-all-done.3.own = bf16[8,256,128]{2,1,0:T(8,128)(2,1)S(1)} async-done(((bf16[8,256,128]{2,1,0:T(8,128)(2,1)}), bf16[8,256,128]{2,1,0:T(8,128)(2,1)S(1)}, u32[]{:S(2)}, u32[]{:S(2)}) %all-to-all-start.3) | async-done | bytes 524320 | tf_op jit(solution)/shard_map/all_to_all | solution.py:64
  122.7 1.1 broadcast_in_dim.16
  123.8 5.5 %all-to-all-start.2 = ((bf16[32,16,1024]{2,1,0:T(8,128)(2,1)}), bf16[32,16,1024]{2,1,0:T(8,128)(2,1)S(1)}, u32[]{:S(2)}, u32[]{:S(2)}) async-start(bf16[32,16,1024]{2,1,0:T(8,128)(2,1)} %broadcast_in_dim.16), calls=%async_computation.2 | async-start | bytes 2097152 | tf_op jit(solution)/shard_map/all_to_all | solution.py:190
  129.3 3.9 %collective-permute-start.6 = (bf16[8,256,128]{2,1,0:T(8,128)(2,1)S(1)}, bf16[8,256,128]{2,1,0:T(8,128)(2,1)S(1)}, u32[]{:S(2)}, u32[]{:S(2)}) collective-permute-start(bf16[8,256,128]{2,1,0:T(8,128)(2,1)S(1)} %all-to-all-done.3.own), channel_id=1, source_target_pairs={{0,1},{1,0},{2,3},{3,2},{4,5},{5,4},{6,7},{7,6},{8,9},{9,8},{10,11... | collective-permute-start | bytes 1572872 | tf_op jit(solution)/shard_map/ppermute | solution.py:171
  133.1 1.5 collective-permute-done.6.other
  135.4 18.6 %all-to-all-done.2 = bf16[32,16,1024]{2,1,0:T(8,128)(2,1)S(1)} async-done(((bf16[32,16,1024]{2,1,0:T(8,128)(2,1)}), bf16[32,16,1024]{2,1,0:T(8,128)(2,1)S(1)}, u32[]{:S(2)}, u32[]{:S(2)}) %all-to-all-start.2) | async-done | bytes 1048608 | tf_op jit(solution)/shard_map/all_to_all | solution.py:190
  156.0 4.2 %collective-permute-start.8 = (bf16[256,128]{1,0:T(8,128)(2,1)S(1)}, bf16[256,128]{1,0:T(8,128)(2,1)S(1)}, u32[]{:S(2)}, u32[]{:S(2)}) collective-permute-start(bf16[256,128]{1,0:T(8,128)(2,1)S(1)} %get-tuple-element.25.own), channel_id=1, source_target_pairs={{0,8},{8,0},{1,9},{9,1},{2,10},{10,2},{3,11},{11,3},{4,12},{12,4},... | collective-permute-start | bytes 196616 | tf_op jit(solution)/shard_map/ppermute | solution.py:185
  160.3 1.6 collective-permute-done.8.other
  162.3 22.7 %all_to_all.30 = bf16[16,16,1024]{2,1,0:T(8,128)(2,1)S(1)} all-to-all(bf16[16,16,1024]{2,1,0:T(8,128)(2,1)S(1)} %bitcast.55), channel_id=1, replica_groups=mesh['gr'=2,'zl'=4,'yh'=4,'yl'=2,'x'=4,'core'=2] {'zl','yh'}, dimensions={0} | all-to-all | bytes 1048576 | tf_op jit(solution)/shard_map/all_to_all | solution.py:187
  185.9 1.1 broadcast_in_dim.37
  187.0 6.2 %all-to-all-start.5 = ((bf16[32,16,1024]{2,1,0:T(8,128)(2,1)}), bf16[32,16,1024]{2,1,0:T(8,128)(2,1)S(1)}, u32[]{:S(2)}, u32[]{:S(2)}) async-start(bf16[32,16,1024]{2,1,0:T(8,128)(2,1)} %broadcast_in_dim.37), calls=%async_computation.5 | async-start | bytes 2097152 | tf_op jit(solution)/shard_map/all_to_all | solution.py:190
  193.2 3.1 %collective-permute-start.7 = (bf16[2,128,1024]{2,1,0:T(8,128)(2,1)S(1)}, bf16[2,128,1024]{2,1,0:T(8,128)(2,1)S(1)}, u32[]{:S(2)}, u32[]{:S(2)}) collective-permute-start(bf16[2,128,1024]{2,1,0:T(8,128)(2,1)S(1)} %get-tuple-element.19.send), channel_id=1, source_target_pairs={{0,8},{8,0},{1,9},{9,1},{2,10},{10,2},{3,11},{11,3},{4,12},{12,4},... | collective-permute-start | bytes 1572872 | tf_op jit(solution)/shard_map/ppermute | solution.py:173
  196.3 32.1 %collective-permute-done.7 = bf16[2,128,1024]{2,1,0:T(8,128)(2,1)S(1)} collective-permute-done((bf16[2,128,1024]{2,1,0:T(8,128)(2,1)S(1)}, bf16[2,128,1024]{2,1,0:T(8,128)(2,1)S(1)}, u32[]{:S(2)}, u32[]{:S(2)}) %collective-permute-start.7) | collective-permute-done | bytes 524320 | tf_op jit(solution)/shard_map/ppermute | solution.py:173
  230.1 1.1 pad_maximum_fusion
  (54 shorter events, 13.3 us)
Async XLA Ops:
  1.7 7.5 %collective-permute-start = (bf16[128,256]{1,0:T(8,128)(2,1)S(1)}, bf16[128,256]{1,0:T(8,128)(2,1)S(1)}, u32[]{:S(2)}, u32[]{:S(2)}) collective-permute-start(bf16[128,256]{1,0:T(8,128)(2,1)S(1)} %pad_maximum_fusion.5), channel_id=1, source_target_pairs={{0,0},{1,16},{2,32},{3,48},{4,64},{5,80},{6,96},{7,112},{8,8},{9,2... | collective-permute-start | bytes 196616 | tf_op jit(solution)/shard_map/ppermute | solution.py:155
  9.3 19.6 %collective-permute-start.1 = (bf16[256,256]{1,0:T(8,128)(2,1)S(1)}, bf16[256,256]{1,0:T(8,128)(2,1)S(1)}, u32[]{:S(2)}, u32[]{:S(2)}) collective-permute-start(bf16[256,256]{1,0:T(8,128)(2,1)S(1)} %maximum_maximum_fusion), channel_id=1, source_target_pairs={{0,256},{256,0},{1,257},{257,1},{2,258},{258,2},{3,259},{259,3},{4... | collective-permute-start | bytes 393224 | tf_op jit(solution)/shard_map/ppermute | solution.py:159
  30.2 31.2 %copy-start = (bf16[1,256,2048]{2,1,0:T(8,128)(2,1)S(1)}, bf16[1,256,2048]{2,1,0:T(8,128)(2,1)}, u32[]{:S(2)}) copy-start(bf16[1,256,2048]{2,1,0:T(8,128)(2,1)} %param.5) | copy-start | bytes 3145732
  30.2 25.5 %all-to-all-start = ((bf16[8,512,128]{2,1,0:T(8,128)(2,1)}), bf16[8,512,128]{2,1,0:T(8,128)(2,1)S(1)}, u32[]{:S(2)}, u32[]{:S(2)}) async-start(bf16[8,512,128]{2,1,0:T(8,128)(2,1)} %bitcast.7), calls=%async_computation | async-start | bytes 2097152 | tf_op jit(solution)/shard_map/all_to_all | solution.py:64
  35.1 9.9 %collective-permute-start.2 = (bf16[128,256]{1,0:T(8,128)(2,1)S(1)}, bf16[128,256]{1,0:T(8,128)(2,1)S(1)}, u32[]{:S(2)}, u32[]{:S(2)}) collective-permute-start(bf16[128,256]{1,0:T(8,128)(2,1)S(1)} %pad_maximum_fusion.6), channel_id=1, source_target_pairs={{0,0},{1,16},{2,32},{3,48},{4,64},{5,80},{6,96},{7,112},{8,8},{9,2... | collective-permute-start | bytes 196616 | tf_op jit(solution)/shard_map/ppermute | solution.py:155
  45.0 10.8 %collective-permute-start.3 = (bf16[128,256]{1,0:T(8,128)(2,1)S(1)}, bf16[128,256]{1,0:T(8,128)(2,1)S(1)}, u32[]{:S(2)}, u32[]{:S(2)}) collective-permute-start(bf16[128,256]{1,0:T(8,128)(2,1)S(1)} %collective-permute-done.2), channel_id=1, source_target_pairs={{0,256},{256,0},{1,257},{257,1},{2,258},{258,2},{3,259},{259,3},{4... | collective-permute-start | bytes 196616 | tf_op jit(solution)/shard_map/ppermute | solution.py:166
  55.8 7.9 %collective-permute-start.4 = (bf16[8,512,128]{2,1,0:T(8,128)(2,1)S(1)}, bf16[8,512,128]{2,1,0:T(8,128)(2,1)S(1)}, u32[]{:S(2)}, u32[]{:S(2)}) collective-permute-start(bf16[8,512,128]{2,1,0:T(8,128)(2,1)S(1)} %all-to-all-done.own), channel_id=1, source_target_pairs={{0,1},{1,0},{2,3},{3,2},{4,5},{5,4},{6,7},{7,6},{8,9},{9,8},{10,11... | collective-permute-start | bytes 3145736 | tf_op jit(solution)/shard_map/ppermute | solution.py:169
  64.4 10.9 %copy-start.1 = (bf16[2048,128]{1,0:T(8,128)(2,1)}, bf16[2048,128]{1,0:T(8,128)(2,1)S(1)}, u32[]{:S(2)}) copy-start(bf16[2048,128]{1,0:T(8,128)(2,1)S(1)} %get-tuple-element.16) | copy-start | bytes 1572868
  64.4 12.8 %collective-permute-start.5 = (bf16[256,128]{1,0:T(8,128)(2,1)S(1)}, bf16[256,128]{1,0:T(8,128)(2,1)S(1)}, u32[]{:S(2)}, u32[]{:S(2)}) collective-permute-start(bf16[256,128]{1,0:T(8,128)(2,1)S(1)} %get-tuple-element.17.own), channel_id=1, source_target_pairs={{0,8},{8,0},{1,9},{9,1},{2,10},{10,2},{3,11},{11,3},{4,12},{12,4},... | collective-permute-start | bytes 196616 | tf_op jit(solution)/shard_map/ppermute | solution.py:185
  78.4 31.4 %all-to-all-start.1 = ((bf16[16,16,1024]{2,1,0:T(8,128)(2,1)}), bf16[16,16,1024]{2,1,0:T(8,128)(2,1)S(1)}, u32[]{:S(2)}, u32[]{:S(2)}) async-start(bf16[16,16,1024]{2,1,0:T(8,128)(2,1)} %bitcast.11), calls=%async_computation.1 | async-start | bytes 1048576 | tf_op jit(solution)/shard_map/all_to_all | solution.py:187
  110.7 12.0 %all-to-all-start.3 = ((bf16[8,256,128]{2,1,0:T(8,128)(2,1)}), bf16[8,256,128]{2,1,0:T(8,128)(2,1)S(1)}, u32[]{:S(2)}, u32[]{:S(2)}) async-start(bf16[8,256,128]{2,1,0:T(8,128)(2,1)} %bitcast.17), calls=%async_computation.3 | async-start | bytes 1048576 | tf_op jit(solution)/shard_map/all_to_all | solution.py:64
  123.8 30.3 %all-to-all-start.2 = ((bf16[32,16,1024]{2,1,0:T(8,128)(2,1)}), bf16[32,16,1024]{2,1,0:T(8,128)(2,1)S(1)}, u32[]{:S(2)}, u32[]{:S(2)}) async-start(bf16[32,16,1024]{2,1,0:T(8,128)(2,1)} %broadcast_in_dim.16), calls=%async_computation.2 | async-start | bytes 2097152 | tf_op jit(solution)/shard_map/all_to_all | solution.py:190
  129.3 5.4 %collective-permute-start.6 = (bf16[8,256,128]{2,1,0:T(8,128)(2,1)S(1)}, bf16[8,256,128]{2,1,0:T(8,128)(2,1)S(1)}, u32[]{:S(2)}, u32[]{:S(2)}) collective-permute-start(bf16[8,256,128]{2,1,0:T(8,128)(2,1)S(1)} %all-to-all-done.3.own), channel_id=1, source_target_pairs={{0,1},{1,0},{2,3},{3,2},{4,5},{5,4},{6,7},{7,6},{8,9},{9,8},{10,11... | collective-permute-start | bytes 1572872 | tf_op jit(solution)/shard_map/ppermute | solution.py:171
  134.7 0.8 copy-start.7
  154.0 1.0 copy-start.8
  156.0 29.0 %copy-start.3 = (bf16[2048,128]{1,0:T(8,128)(2,1)}, bf16[2048,128]{1,0:T(8,128)(2,1)S(1)}, u32[]{:S(2)}) copy-start(bf16[2048,128]{1,0:T(8,128)(2,1)S(1)} %get-tuple-element.24) | copy-start | bytes 1572868
  156.0 29.0 %copy-start.5 = (bf16[2048,128]{1,0:T(8,128)(2,1)}, bf16[2048,128]{1,0:T(8,128)(2,1)S(1)}, u32[]{:S(2)}) copy-start(bf16[2048,128]{1,0:T(8,128)(2,1)S(1)} %get-tuple-element.22) | copy-start | bytes 1572868
  156.0 5.9 %collective-permute-start.8 = (bf16[256,128]{1,0:T(8,128)(2,1)S(1)}, bf16[256,128]{1,0:T(8,128)(2,1)S(1)}, u32[]{:S(2)}, u32[]{:S(2)}) collective-permute-start(bf16[256,128]{1,0:T(8,128)(2,1)S(1)} %get-tuple-element.25.own), channel_id=1, source_target_pairs={{0,8},{8,0},{1,9},{9,1},{2,10},{10,2},{3,11},{11,3},{4,12},{12,4},... | collective-permute-start | bytes 196616 | tf_op jit(solution)/shard_map/ppermute | solution.py:185
  187.0 45.4 %all-to-all-start.5 = ((bf16[32,16,1024]{2,1,0:T(8,128)(2,1)}), bf16[32,16,1024]{2,1,0:T(8,128)(2,1)S(1)}, u32[]{:S(2)}, u32[]{:S(2)}) async-start(bf16[32,16,1024]{2,1,0:T(8,128)(2,1)} %broadcast_in_dim.37), calls=%async_computation.5 | async-start | bytes 2097152 | tf_op jit(solution)/shard_map/all_to_all | solution.py:190
  193.2 35.3 %collective-permute-start.7 = (bf16[2,128,1024]{2,1,0:T(8,128)(2,1)S(1)}, bf16[2,128,1024]{2,1,0:T(8,128)(2,1)S(1)}, u32[]{:S(2)}, u32[]{:S(2)}) collective-permute-start(bf16[2,128,1024]{2,1,0:T(8,128)(2,1)S(1)} %get-tuple-element.19.send), channel_id=1, source_target_pairs={{0,8},{8,0},{1,9},{9,1},{2,10},{10,2},{3,11},{11,3},{4,12},{12,4},... | collective-permute-start | bytes 1572872 | tf_op jit(solution)/shard_map/ppermute | solution.py:173
  228.5 1.1 copy-start.2
  228.6 1.6 copy-start.6
  230.1 1.2 copy-start.4

commit v5 on v4

v5 whole, which is shorter than its diff:
```python
import jax
import jax.numpy as jnp
from jax import lax
from jax.experimental import pallas as pl
from jax.experimental.pallas import tpu as pltpu
from jax.sharding import Mesh
from jax.sharding import PartitionSpec as P


norm_eps = 1e-06
bf16 = jnp.bfloat16
f32 = jnp.float32

AXES = ("gr", "zl", "yh", "yl", "x", "core")
SIZES = (2, 4, 4, 2, 4, 2)
FS = ("zl", "yh", "yl")
GT = ("gr", "x", "core")
SWAP = [(0, 1), (1, 0)]


def device(gr, fs, tp):
    return gr * 256 + fs * 8 + tp


def everyone():
    return [(gr, fs, tp) for gr in range(2) for fs in range(32) for tp in range(8)]


def weight_moves():
    moves = []
    for gr, fs, tp in everyone():
        to = device(fs >> 4, 2 * (8 * gr + tp) + (fs & 1), (fs >> 1) & 7)
        moves.append((device(gr, fs, tp), to))
    return moves


def in_vmem(value):
    return pltpu.with_memory_space_constraint(value, pltpu.VMEM)


def kernel(body, outs, scratch=()):
    here = pl.BlockSpec(memory_space=pltpu.VMEM)

    def call(*args):
        return pl.pallas_call(
            body,
            in_specs=[here] * len(args),
            out_specs=tuple(here for _ in outs),
            out_shape=tuple(pltpu.VMEM(shape, bf16) for shape in outs),
            scratch_shapes=[pltpu.VMEM(shape, bf16) for shape in scratch],
            compiler_params=pltpu.CompilerParams(vmem_limit_bytes=16 << 20),
        )(*[in_vmem(a) for a in args])

    return call


def in_order(first, second, swapped):
    return jnp.where(swapped, second, first), jnp.where(swapped, first, second)


def to_everyone(value, axes, count):
    return lax.all_to_all(
        jnp.broadcast_to(value[None], (count, *value.shape)), axes, 0, 0, tiled=True
    )


def halves_to_all(blocks):
    rows = blocks[0].shape[0]
    sends = jnp.broadcast_to(jnp.stack(blocks)[None], (4, 2, rows, 128)).reshape(8, rows, 128)
    return lax.all_to_all(sends, ("x", "yl"), 0, 0, tiled=True)


def columns(rows, b):
    return [r[:, 128 * b : 128 * b + 128] for r in rows]


def gather_rows(core, own, other, both):
    mine = core == 0
    width = both.shape[1] // 2
    for x in range(4):
        for b in range(2):
            for s in range(2):
                mn = own[2 * x + b, 128 * s : 128 * s + 128]
                ot = other[2 * x + b, 128 * s : 128 * s + 128]
                for c in range(2):
                    line = jnp.where(mine, mn, ot) if c == 0 else jnp.where(mine, ot, mn)
                    at = 64 * (16 * s + 4 * x + 2 * c + b)
                    both[at : at + 64, :width] = line[:64]
                    both[at : at + 64, width:] = line[64:]


def gated(act):
    width = act.shape[1] // 2
    gate_act, up_act = act[:, :width], act[:, width:]
    return (gate_act / (1.0 + jnp.exp(-gate_act)) * up_act).astype(bf16)


def early_up_call(normed, own, other):
    def body(normed, own, other, gate, up, hidden, both):
        gather_rows(lax.axis_index("core"), own, other, both)
        gate[...] = both[:, :128]
        up[...] = both[:, 128:]
        hidden[...] = gated(jnp.dot(normed[...], both[...], preferred_element_type=f32))

    outs = ((2048, 128), (2048, 128), (256, 128))
    return kernel(body, outs, ((2048, 256),))(normed, own, other)


def late_up_call(stream, own, other):
    def body(stream, own, other, gate, up, hidden, both):
        gather_rows(lax.axis_index("core"), own, other, both)
        even = lax.axis_index("yl") == 0
        gate[...] = jnp.where(even, both[:, :128], both[:, 128:256])
        up[...] = jnp.where(even, both[:, 256:384], both[:, 384:])
        squares = jnp.zeros((128, 1), f32)
        for z in range(2):
            part = stream[z].astype(f32)
            squares = squares + jnp.sum(part * part, axis=1, keepdims=True)
        scale = lax.rsqrt(squares * (1.0 / 2048) + norm_eps)
        act = jnp.zeros((128, 512), f32)
        for z in range(2):
            part = (stream[z].astype(f32) * scale).astype(bf16)
            rows = both[1024 * z : 1024 * z + 1024]
            act = act + jnp.dot(part, rows, preferred_element_type=f32)
        hidden[...] = gated(act)

    outs = ((2048, 128), (2048, 128), (128, 256))
    return kernel(body, outs, ((2048, 512),))(stream, own, other)


def norm_call(stream):
    def body(stream, out):
        value = stream[...].astype(f32)
        mean = jnp.sum(value * value, axis=1, keepdims=True) * (1.0 / 2048)
        out[...] = (value * lax.rsqrt(mean + norm_eps)).astype(bf16)

    return kernel(body, ((256, 2048),))(stream)[0]


def down_rows_call(own, other):
    def body(own, other, keep, send, pair, one):
        mine = lax.axis_index("core") == 0
        even = lax.axis_index("yl") == 0
        for x in range(4):
            for k in range(3):
                at = 256 + 128 * k
                mn = [own[2 * x + b, at : at + 128] for b in range(2)]
                ot = [other[2 * x + b, at : at + 128] for b in range(2)]
                for c in range(2):
                    a, b = (mn, ot) if c == 0 else (ot, mn)
                    line = [jnp.where(mine, a[i], b[i]) for i in range(2)]
                    col = 256 * x + 128 * c
                    if k == 0:
                        keep[:, col : col + 128] = jnp.where(even, line[0], line[1])
                        send[:, col : col + 128] = jnp.where(even, line[1], line[0])
                    else:
                        col = col + 1024 * (k - 1)
                        one[:, col : col + 128] = jnp.where(even, line[0], line[1])
                        pair[:128, col : col + 128] = line[0]
                        pair[128:, col : col + 128] = line[1]

    outs = ((128, 1024), (128, 1024), (256, 2048), (128, 2048))
    return kernel(body, outs)(own, other)


def early_down_call(own, other, keep, send):
    def body(own, other, keep, send, out):
        act = jnp.dot(own[...], keep[...], preferred_element_type=f32)
        act = act + jnp.dot(other[...], send[...], preferred_element_type=f32)
        out[...] = act.astype(bf16)

    return kernel(body, ((256, 1024),))(own, other, keep, send)[0]


def late_down_call(hidden, pair):
    def body(hidden, pair, out):
        out[...] = jnp.dot(hidden[...], pair[...], preferred_element_type=f32).astype(bf16)

    return kernel(body, ((128, 2048),))(hidden, pair)[0]


def step(prompt, norm_gain, gate_weight, up_weight, down_weight):
    gain = norm_gain[:, :, None]
    gate = (gain * gate_weight).astype(bf16)
    up = (gain * up_weight).astype(bf16)
    high = lax.axis_index("gr") == 1
    moved = []
    for layer in range(2):
        block = jnp.concatenate([gate[layer], up[layer]], axis=0)
        moved.append(lax.ppermute(block, AXES, weight_moves()))
    down = down_weight.astype(bf16)
    down = jnp.concatenate([down[0], down[1]], axis=1)
    both = jnp.concatenate([moved[0], down], axis=0)
    across = lax.ppermute(both, "gr", SWAP)
    rows = in_order(both, across, high)
    blocks = []
    for b in range(2):
        lower = [rows[b][128:, :128], rows[0][128:, 128:], rows[1][128:, 128:]]
        blocks.append(jnp.concatenate([*columns([r[:128] for r in rows], b), *lower]))
    own = halves_to_all(blocks)
    across = lax.ppermute(moved[1], "gr", SWAP)
    own, *late = lax.optimization_barrier((own, moved[1], across))
    rows = in_order(*late, high)
    early = own, lax.ppermute(own, "core", SWAP)
    own = to_everyone(jnp.concatenate(rows), ("x", "yl"), 8)
    late = own, lax.ppermute(own, "core", SWAP)
    keep, send, pair, one = down_rows_call(*early)
    came = lax.ppermute(send, "yl", SWAP)

    yl = lax.axis_index("yl")
    odd = yl == 1
    normed = norm_call(prompt[0])
    gate0, up0, hidden = early_up_call(normed, *early)
    other = lax.ppermute(hidden, "yl", SWAP)
    part = early_down_call(hidden, other, keep, send)
    parts = lax.all_to_all(part.reshape(16, 16, 1024), ("zl", "yh"), 0, 0, tiled=True)
    start = lax.axis_index(("zl", "yh")) * 16, yl * 1024
    mine = lax.dynamic_slice(prompt[0], start, (16, 1024)).astype(f32)
    mine = mine + 0.5 * jnp.sum(parts.astype(f32), axis=0)
    sends = mine.astype(bf16).reshape(2, 1, 8, 1024)
    sends = jnp.broadcast_to(sends, (2, 16, 8, 1024)).reshape(32, 8, 1024)
    stream = lax.all_to_all(sends, ("yl", "zl", "yh"), 0, 0, tiled=True)
    kept, sent = in_order(mine[:8], mine[8:], odd)
    rest = lax.ppermute(sent, "yl", SWAP)
    mine = jnp.concatenate(in_order(kept, rest, odd), axis=1)
    gate1, up1, hidden = late_up_call(stream.reshape(2, 128, 1024), *late)
    part = late_down_call(hidden, pair)
    parts = lax.all_to_all(part.reshape(16, 8, 2048), ("zl", "yh"), 0, 0, tiled=True)
    mine = mine + 0.5 * jnp.sum(parts.astype(f32), axis=0)
    mixed = to_everyone(mine.astype(bf16), FS, 32)
    served = jnp.stack([jnp.concatenate(in_order(keep, came, odd), axis=1), one])
    gates, ups = jnp.stack([gate0, gate1]), jnp.stack([up0, up1])
    return gates, ups, served, mixed.reshape(prompt.shape)


def solution(mesh):
    fine = Mesh(mesh.devices.reshape(SIZES), AXES)
    in_specs = (P(GT, None, None), P(None, FS), P(None, FS, GT), P(None, FS, GT), P(None, FS, GT))
    out_specs = (P(None, None, FS), P(None, None, FS), P(None, FS, None), P(GT, None, None))
    return jax.shard_map(step, mesh=fine, in_specs=in_specs, out_specs=out_specs, check_vma=False)
```

time: 235 us -> 211 us (0.90)
  the two profiles are of different devices: /device:TPU:1 before, /device:TPU:2 now
where the time goes in v5:
time: 211 us; the launch traced here: 210 us
  waiting for transfers between devices  99.1 us (47%)
  starting transfers between devices  86.6 us (41%)
  local copies, waits for them, and re-layouts  11.4 us (5%)
  Pallas kernels  6.22 us (3%)
  other arithmetic  5.6 us (3%)
    ppermute x1, waiting for transfers between devices, step(): came = lax.ppermute(send, 'yl', SWAP)  25.1 us
    all_to_all x1, waiting for transfers between devices, step(): stream = lax.all_to_all(sends, ('yl', 'zl', 'yh'), 0, 0, tiled=True)  17.5 us
    all_to_all x1, waiting for transfers between devices, step(): lax.all_to_all(part.reshape(16, 16, 1024), ('zl', 'yh'), 0, 0, tiled=True)  16.9 us
    ppermute x1, starting transfers between devices, step(): across = lax.ppermute(both, 'gr', SWAP)  14.7 us
    ppermute x2, waiting for transfers between devices, step(): moved.append(lax.ppermute(block, AXES, weight_moves()))  14.3 us
    all_to_all x2, starting transfers between devices, to_everyone(): lax.all_to_all(jnp.broadcast_to(value[None], (count, *value.shape)), axes...  12.8 us
    ppermute x2, starting transfers between devices, step(): moved.append(lax.ppermute(block, AXES, weight_moves()))  12.5 us
    ppermute x1, waiting for transfers between devices, step(): rest = lax.ppermute(sent, 'yl', SWAP)  9.53 us
  transfers between devices with their start and end apart: 15, of which 11 were waited for; matrix products, arithmetic and copies ran while one was open for 2% of the time, Pallas kernels for 1%

profile of v5, /device:TPU:2, one launch (start us, length us, event | category | flops | bytes accessed | tf_op | source)
XLA Modules:
  0.0 209.9 jit_solution(3444835056669338675)
XLA Ops:
  0.6 1.1 multiply_convert_fusion.1
  1.7 7.7 %collective-permute-start = (bf16[128,256]{1,0:T(8,128)(2,1)S(1)}, bf16[128,256]{1,0:T(8,128)(2,1)S(1)}, u32[]{:S(2)}, u32[]{:S(2)}) collective-permute-start(bf16[128,256]{1,0:T(8,128)(2,1)S(1)} %pad_maximum_fusion.5), channel_id=1, source_target_pairs={{0,0},{1,16},{2,32},{3,48},{4,64},{5,80},{6,96},{7,112},{8,8},{9,2... | collective-permute-start | bytes 196616 | tf_op jit(solution)/shard_map/ppermute | solution.py:190
  10.4 2.3 %collective-permute-done = bf16[128,256]{1,0:T(8,128)(2,1)S(1)} collective-permute-done((bf16[128,256]{1,0:T(8,128)(2,1)S(1)}, bf16[128,256]{1,0:T(8,128)(2,1)S(1)}, u32[]{:S(2)}, u32[]{:S(2)}) %collective-permute-start) | collective-permute-done | bytes 65568 | tf_op jit(solution)/shard_map/ppermute | solution.py:190
  12.7 14.7 %collective-permute-start.1 = (bf16[256,256]{1,0:T(8,128)(2,1)S(1)}, bf16[256,256]{1,0:T(8,128)(2,1)S(1)}, u32[]{:S(2)}, u32[]{:S(2)}) collective-permute-start(bf16[256,256]{1,0:T(8,128)(2,1)S(1)} %maximum_maximum_fusion), channel_id=1, source_target_pairs={{0,256},{256,0},{1,257},{257,1},{2,258},{258,2},{3,259},{259,3},{4... | collective-permute-start | bytes 393224 | tf_op jit(solution)/shard_map/ppermute | solution.py:194
  27.5 3.2 %collective-permute-done.1 = bf16[256,256]{1,0:T(8,128)(2,1)S(1)} collective-permute-done((bf16[256,256]{1,0:T(8,128)(2,1)S(1)}, bf16[256,256]{1,0:T(8,128)(2,1)S(1)}, u32[]{:S(2)}, u32[]{:S(2)}) %collective-permute-start.1) | collective-permute-done | bytes 131104 | tf_op jit(solution)/shard_map/ppermute | solution.py:194
  30.9 1.3 broadcast_in_dim.8
  32.2 7.6 %all-to-all-start = ((bf16[8,640,128]{2,1,0:T(8,128)(2,1)}), bf16[8,640,128]{2,1,0:T(8,128)(2,1)S(1)}, u32[]{:S(2)}, u32[]{:S(2)}) async-start(bf16[8,640,128]{2,1,0:T(8,128)(2,1)} %bitcast.7), calls=%async_computation | async-start | bytes 2621440 | tf_op jit(solution)/shard_map/all_to_all | solution.py:70
  39.7 4.8 %collective-permute-start.2 = (bf16[128,256]{1,0:T(8,128)(2,1)S(1)}, bf16[128,256]{1,0:T(8,128)(2,1)S(1)}, u32[]{:S(2)}, u32[]{:S(2)}) collective-permute-start(bf16[128,256]{1,0:T(8,128)(2,1)S(1)} %pad_maximum_fusion.6), channel_id=1, source_target_pairs={{0,0},{1,16},{2,32},{3,48},{4,64},{5,80},{6,96},{7,112},{8,8},{9,2... | collective-permute-start | bytes 196616 | tf_op jit(solution)/shard_map/ppermute | solution.py:190
  44.5 11.9 %collective-permute-done.2 = bf16[128,256]{1,0:T(8,128)(2,1)S(1)} collective-permute-done((bf16[128,256]{1,0:T(8,128)(2,1)S(1)}, bf16[128,256]{1,0:T(8,128)(2,1)S(1)}, u32[]{:S(2)}, u32[]{:S(2)}) %collective-permute-start.2) | collective-permute-done | bytes 65568 | tf_op jit(solution)/shard_map/ppermute | solution.py:190
  56.5 8.9 %collective-permute-start.3 = (bf16[128,256]{1,0:T(8,128)(2,1)S(1)}, bf16[128,256]{1,0:T(8,128)(2,1)S(1)}, u32[]{:S(2)}, u32[]{:S(2)}) collective-permute-start(bf16[128,256]{1,0:T(8,128)(2,1)S(1)} %collective-permute-done.2), channel_id=1, source_target_pairs={{0,256},{256,0},{1,257},{257,1},{2,258},{258,2},{3,259},{259,3},{4... | collective-permute-start | bytes 196616 | tf_op jit(solution)/shard_map/ppermute | solution.py:201
  65.4 2.2 %collective-permute-done.3 = bf16[128,256]{1,0:T(8,128)(2,1)S(1)} collective-permute-done((bf16[128,256]{1,0:T(8,128)(2,1)S(1)}, bf16[128,256]{1,0:T(8,128)(2,1)S(1)}, u32[]{:S(2)}, u32[]{:S(2)}) %collective-permute-start.3) | collective-permute-done | bytes 65568 | tf_op jit(solution)/shard_map/ppermute | solution.py:201
  68.7 8.8 %all-to-all-start.3 = ((bf16[8,256,256]{2,1,0:T(8,128)(2,1)}), bf16[8,256,256]{2,1,0:T(8,128)(2,1)S(1)}, u32[]{:S(2)}, u32[]{:S(2)}) async-start(bf16[8,256,256]{2,1,0:T(8,128)(2,1)} %broadcast_in_dim.10), calls=%async_computation.3 | async-start | bytes 2097152 | tf_op jit(solution)/shard_map/all_to_all | solution.py:62
  77.5 1.9 collective-permute-start.4
  79.8 2.6 %collective-permute-done.4.other = bf16[8,640,128]{2,1,0:T(8,128)(2,1)S(1)} collective-permute-done((bf16[8,640,128]{2,1,0:T(8,128)(2,1)S(1)}, bf16[8,640,128]{2,1,0:T(8,128)(2,1)S(1)}, u32[]{:S(2)}, u32[]{:S(2)}) %collective-permute-start.4) | collective-permute-done | bytes 1310752 | tf_op jit(solution)/shard_map/ppermute | solution.py:204
  84.7 3.4 %collective-permute-start.5 = (bf16[256,128]{1,0:T(8,128)(2,1)S(1)}, bf16[256,128]{1,0:T(8,128)(2,1)S(1)}, u32[]{:S(2)}, u32[]{:S(2)}) collective-permute-start(bf16[256,128]{1,0:T(8,128)(2,1)S(1)} %get-tuple-element.19.own), channel_id=1, source_target_pairs={{0,8},{8,0},{1,9},{9,1},{2,10},{10,2},{3,11},{11,3},{4,12},{12,4},... | collective-permute-start | bytes 196616 | tf_op jit(solution)/shard_map/ppermute | solution.py:214
  90.5 1.5 collective-permute-done.5.other
  92.0 1.2 shard_map.87
  94.6 8.0 %all-to-all-start.1 = ((bf16[16,16,1024]{2,1,0:T(8,128)(2,1)}), bf16[16,16,1024]{2,1,0:T(8,128)(2,1)S(1)}, u32[]{:S(2)}, u32[]{:S(2)}) async-start(bf16[16,16,1024]{2,1,0:T(8,128)(2,1)} %bitcast.12), calls=%async_computation.1 | async-start | bytes 1048576 | tf_op jit(solution)/shard_map/all_to_all | solution.py:216
  102.6 1.9 collective-permute-start.6
  104.6 16.9 %all-to-all-done.1 = bf16[16,16,1024]{2,1,0:T(8,128)(2,1)S(1)} async-done(((bf16[16,16,1024]{2,1,0:T(8,128)(2,1)}), bf16[16,16,1024]{2,1,0:T(8,128)(2,1)S(1)}, u32[]{:S(2)}, u32[]{:S(2)}) %all-to-all-start.1) | async-done | bytes 524320 | tf_op jit(solution)/shard_map/all_to_all | solution.py:216
  122.5 3.9 %all-to-all-start.2 = ((bf16[32,8,1024]{2,1,0:T(8,128)(2,1)}), bf16[32,8,1024]{2,1,0:T(8,128)(2,1)S(1)}, u32[]{:S(2)}, u32[]{:S(2)}) async-start(bf16[32,8,1024]{2,1,0:T(8,128)(2,1)} %bitcast.14), calls=%async_computation.2 | async-start | bytes 1048576 | tf_op jit(solution)/shard_map/all_to_all | solution.py:222
  126.4 17.5 %all-to-all-done.2 = bf16[32,8,1024]{2,1,0:T(8,128)(2,1)S(1)} async-done(((bf16[32,8,1024]{2,1,0:T(8,128)(2,1)}), bf16[32,8,1024]{2,1,0:T(8,128)(2,1)S(1)}, u32[]{:S(2)}, u32[]{:S(2)}) %all-to-all-start.2) | async-done | bytes 524320 | tf_op jit(solution)/shard_map/all_to_all | solution.py:222
  143.9 2.3 %shard_map.88 = (bf16[2048,128]{1,0:T(8,128)(2,1)S(1)}, bf16[2048,128]{1,0:T(8,128)(2,1)S(1)}, bf16[128,256]{1,0:T(8,128)(2,1)S(1)}) custom-call(bf16[2,128,1024]{2,1,0:T(8,128)(2,1)S(1)} %bitcast.40, bf16[8,256,256]{2,1,0:T(8,128)(2,1)S(1)} %all-to-all-done.3.own, bf16[8,256,256]{2,1,0:T(8,128)(2,1)} %collective-permute-done.6.other), custom_call_target="tpu_custom_call" | custom-call | tf_op jit(solution)/shard_map/pallas_call | solution.py:45
  147.0 1.1 shard_map.89
  148.1 4.0 %all-to-all-start.4 = ((bf16[16,8,2048]{2,1,0:T(8,128)(2,1)}), bf16[16,8,2048]{2,1,0:T(8,128)(2,1)S(1)}, u32[]{:S(2)}, u32[]{:S(2)}) async-start(bf16[16,8,2048]{2,1,0:T(8,128)(2,1)} %bitcast.22), calls=%async_computation.4 | async-start | bytes 1048576 | tf_op jit(solution)/shard_map/all_to_all | solution.py:228
  152.1 3.3 %collective-permute-start.8 = (f32[8,1024]{1,0:T(8,128)S(1)}, f32[8,1024]{1,0:T(8,128)S(1)}, u32[]{:S(2)}, u32[]{:S(2)}) collective-permute-start(f32[8,1024]{1,0:T(8,128)S(1)} %slice_select_fusion.1), channel_id=1, source_target_pairs={{0,8},{8,0},{1,9},{9,1},{2,10},{10,2},{3,11},{11,3},{4,12},{12,4},... | collective-permute-start | bytes 98312 | tf_op jit(solution)/shard_map/ppermute | solution.py:224
  155.4 9.5 %collective-permute-done.8 = f32[8,1024]{1,0:T(8,128)S(1)} collective-permute-done((f32[8,1024]{1,0:T(8,128)S(1)}, f32[8,1024]{1,0:T(8,128)S(1)}, u32[]{:S(2)}, u32[]{:S(2)}) %collective-permute-start.8) | collective-permute-done | bytes 32800 | tf_op jit(solution)/shard_map/ppermute | solution.py:224
  164.9 6.2 %all-to-all-done.4 = bf16[16,8,2048]{2,1,0:T(8,128)(2,1)S(1)} async-done(((bf16[16,8,2048]{2,1,0:T(8,128)(2,1)}), bf16[16,8,2048]{2,1,0:T(8,128)(2,1)S(1)}, u32[]{:S(2)}, u32[]{:S(2)}) %all-to-all-start.4) | async-done | bytes 524320 | tf_op jit(solution)/shard_map/all_to_all | solution.py:228
  171.2 1.1 broadcast_in_dim.11
  172.3 4.1 %all-to-all-start.5 = ((bf16[32,8,2048]{2,1,0:T(8,128)(2,1)}), bf16[32,8,2048]{2,1,0:T(8,128)(2,1)S(1)}, u32[]{:S(2)}, u32[]{:S(2)}) async-start(bf16[32,8,2048]{2,1,0:T(8,128)(2,1)} %broadcast_in_dim.11), calls=%async_computation.5 | async-start | bytes 2097152 | tf_op jit(solution)/shard_map/all_to_all | solution.py:62
  176.4 3.7 %collective-permute-start.7 = (bf16[128,1024]{1,0:T(8,128)(2,1)S(1)}, bf16[128,1024]{1,0:T(8,128)(2,1)S(1)}, u32[]{:S(2)}, u32[]{:S(2)}) collective-permute-start(bf16[128,1024]{1,0:T(8,128)(2,1)S(1)} %copy-done.14), channel_id=1, source_target_pairs={{0,8},{8,0},{1,9},{9,1},{2,10},{10,2},{3,11},{11,3},{4,12},{12,4},... | collective-permute-start | bytes 786440 | tf_op jit(solution)/shard_map/ppermute | solution.py:208
  180.1 25.1 %collective-permute-done.7 = bf16[128,1024]{1,0:T(8,128)(2,1)S(1)} collective-permute-done((bf16[128,1024]{1,0:T(8,128)(2,1)S(1)}, bf16[128,1024]{1,0:T(8,128)(2,1)S(1)}, u32[]{:S(2)}, u32[]{:S(2)}) %collective-permute-start.7) | collective-permute-done | bytes 262176 | tf_op jit(solution)/shard_map/ppermute | solution.py:208
  (69 shorter events, 15.2 us)
Async XLA Ops:
  1.7 11.0 %collective-permute-start = (bf16[128,256]{1,0:T(8,128)(2,1)S(1)}, bf16[128,256]{1,0:T(8,128)(2,1)S(1)}, u32[]{:S(2)}, u32[]{:S(2)}) collective-permute-start(bf16[128,256]{1,0:T(8,128)(2,1)S(1)} %pad_maximum_fusion.5), channel_id=1, source_target_pairs={{0,0},{1,16},{2,32},{3,48},{4,64},{5,80},{6,96},{7,112},{8,8},{9,2... | collective-permute-start | bytes 196616 | tf_op jit(solution)/shard_map/ppermute | solution.py:190
  12.7 18.0 %collective-permute-start.1 = (bf16[256,256]{1,0:T(8,128)(2,1)S(1)}, bf16[256,256]{1,0:T(8,128)(2,1)S(1)}, u32[]{:S(2)}, u32[]{:S(2)}) collective-permute-start(bf16[256,256]{1,0:T(8,128)(2,1)S(1)} %maximum_maximum_fusion), channel_id=1, source_target_pairs={{0,256},{256,0},{1,257},{257,1},{2,258},{258,2},{3,259},{259,3},{4... | collective-permute-start | bytes 393224 | tf_op jit(solution)/shard_map/ppermute | solution.py:194
  32.2 35.5 %all-to-all-start = ((bf16[8,640,128]{2,1,0:T(8,128)(2,1)}), bf16[8,640,128]{2,1,0:T(8,128)(2,1)S(1)}, u32[]{:S(2)}, u32[]{:S(2)}) async-start(bf16[8,640,128]{2,1,0:T(8,128)(2,1)} %bitcast.7), calls=%async_computation | async-start | bytes 2621440 | tf_op jit(solution)/shard_map/all_to_all | solution.py:70
  39.7 16.8 %collective-permute-start.2 = (bf16[128,256]{1,0:T(8,128)(2,1)S(1)}, bf16[128,256]{1,0:T(8,128)(2,1)S(1)}, u32[]{:S(2)}, u32[]{:S(2)}) collective-permute-start(bf16[128,256]{1,0:T(8,128)(2,1)S(1)} %pad_maximum_fusion.6), channel_id=1, source_target_pairs={{0,0},{1,16},{2,32},{3,48},{4,64},{5,80},{6,96},{7,112},{8,8},{9,2... | collective-permute-start | bytes 196616 | tf_op jit(solution)/shard_map/ppermute | solution.py:190
  56.5 11.2 %collective-permute-start.3 = (bf16[128,256]{1,0:T(8,128)(2,1)S(1)}, bf16[128,256]{1,0:T(8,128)(2,1)S(1)}, u32[]{:S(2)}, u32[]{:S(2)}) collective-permute-start(bf16[128,256]{1,0:T(8,128)(2,1)S(1)} %collective-permute-done.2), channel_id=1, source_target_pairs={{0,256},{256,0},{1,257},{257,1},{2,258},{258,2},{3,259},{259,3},{4... | collective-permute-start | bytes 196616 | tf_op jit(solution)/shard_map/ppermute | solution.py:201
  68.7 10.7 %copy-start = (bf16[1,256,2048]{2,1,0:T(8,128)(2,1)S(1)}, bf16[1,256,2048]{2,1,0:T(8,128)(2,1)}, u32[]{:S(2)}) copy-start(bf16[1,256,2048]{2,1,0:T(8,128)(2,1)} %param.5) | copy-start | bytes 3145732
  68.7 25.9 %all-to-all-start.3 = ((bf16[8,256,256]{2,1,0:T(8,128)(2,1)}), bf16[8,256,256]{2,1,0:T(8,128)(2,1)S(1)}, u32[]{:S(2)}, u32[]{:S(2)}) async-start(bf16[8,256,256]{2,1,0:T(8,128)(2,1)} %broadcast_in_dim.10), calls=%async_computation.3 | async-start | bytes 2097152 | tf_op jit(solution)/shard_map/all_to_all | solution.py:62
  77.5 4.9 %collective-permute-start.4 = (bf16[8,640,128]{2,1,0:T(8,128)(2,1)S(1)}, bf16[8,640,128]{2,1,0:T(8,128)(2,1)S(1)}, u32[]{:S(2)}, u32[]{:S(2)}) collective-permute-start(bf16[8,640,128]{2,1,0:T(8,128)(2,1)S(1)} %all-to-all-done.own), channel_id=1, source_target_pairs={{0,1},{1,0},{2,3},{3,2},{4,5},{5,4},{6,7},{7,6},{8,9},{9,8},{10,11... | collective-permute-start | bytes 3932168 | tf_op jit(solution)/shard_map/ppermute | solution.py:204
  83.1 0.8 copy-start.5
  83.9 0.8 copy-start.7
  84.7 7.3 %collective-permute-start.5 = (bf16[256,128]{1,0:T(8,128)(2,1)S(1)}, bf16[256,128]{1,0:T(8,128)(2,1)S(1)}, u32[]{:S(2)}, u32[]{:S(2)}) collective-permute-start(bf16[256,128]{1,0:T(8,128)(2,1)S(1)} %get-tuple-element.19.own), channel_id=1, source_target_pairs={{0,8},{8,0},{1,9},{9,1},{2,10},{10,2},{3,11},{11,3},{4,12},{12,4},... | collective-permute-start | bytes 196616 | tf_op jit(solution)/shard_map/ppermute | solution.py:214
  88.7 1.0 copy-start.1
  89.7 0.8 copy-start.9
  93.2 0.7 copy-start.3
  93.9 0.7 copy-start.13
  94.6 26.9 %all-to-all-start.1 = ((bf16[16,16,1024]{2,1,0:T(8,128)(2,1)}), bf16[16,16,1024]{2,1,0:T(8,128)(2,1)S(1)}, u32[]{:S(2)}, u32[]{:S(2)}) async-start(bf16[16,16,1024]{2,1,0:T(8,128)(2,1)} %bitcast.12), calls=%async_computation.1 | async-start | bytes 1048576 | tf_op jit(solution)/shard_map/all_to_all | solution.py:216
  102.6 23.7 %collective-permute-start.6 = (bf16[8,256,256]{2,1,0:T(8,128)(2,1)S(1)}, bf16[8,256,256]{2,1,0:T(8,128)(2,1)}, u32[]{:S(2)}, u32[]{:S(2)}) collective-permute-start(bf16[8,256,256]{2,1,0:T(8,128)(2,1)S(1)} %all-to-all-done.3.own), channel_id=1, source_target_pairs={{0,1},{1,0},{2,3},{3,2},{4,5},{5,4},{6,7},{7,6},{8,9},{9,8},{10,11... | collective-permute-start | bytes 3145736 | tf_op jit(solution)/shard_map/ppermute | solution.py:206
  122.5 21.4 %all-to-all-start.2 = ((bf16[32,8,1024]{2,1,0:T(8,128)(2,1)}), bf16[32,8,1024]{2,1,0:T(8,128)(2,1)S(1)}, u32[]{:S(2)}, u32[]{:S(2)}) async-start(bf16[32,8,1024]{2,1,0:T(8,128)(2,1)} %bitcast.14), calls=%async_computation.2 | async-start | bytes 1048576 | tf_op jit(solution)/shard_map/all_to_all | solution.py:222
  143.9 3.1 %copy-start.2 = (bf16[256,2048]{1,0:T(8,128)(2,1)S(1)}, bf16[256,2048]{1,0:T(8,128)(2,1)}, u32[]{:S(2)}) copy-start(bf16[256,2048]{1,0:T(8,128)(2,1)} %copy-done.1) | copy-start | bytes 3145732
  146.2 0.8 copy-start.11
  148.1 23.0 %all-to-all-start.4 = ((bf16[16,8,2048]{2,1,0:T(8,128)(2,1)}), bf16[16,8,2048]{2,1,0:T(8,128)(2,1)S(1)}, u32[]{:S(2)}, u32[]{:S(2)}) async-start(bf16[16,8,2048]{2,1,0:T(8,128)(2,1)} %bitcast.22), calls=%async_computation.4 | async-start | bytes 1048576 | tf_op jit(solution)/shard_map/all_to_all | solution.py:228
  152.1 12.8 %collective-permute-start.8 = (f32[8,1024]{1,0:T(8,128)S(1)}, f32[8,1024]{1,0:T(8,128)S(1)}, u32[]{:S(2)}, u32[]{:S(2)}) collective-permute-start(f32[8,1024]{1,0:T(8,128)S(1)} %slice_select_fusion.1), channel_id=1, source_target_pairs={{0,8},{8,0},{1,9},{9,1},{2,10},{10,2},{3,11},{11,3},{4,12},{12,4},... | collective-permute-start | bytes 98312 | tf_op jit(solution)/shard_map/ppermute | solution.py:224
  172.3 4.1 %copy-start.14 = (bf16[128,1024]{1,0:T(8,128)(2,1)S(1)}, bf16[128,1024]{1,0:T(8,128)(2,1)}, u32[]{:S(2)}) copy-start(bf16[128,1024]{1,0:T(8,128)(2,1)} %copy-done.13) | copy-start | bytes 786436
  172.3 32.9 %copy-start.4 = (bf16[128,1024]{1,0:T(8,128)(2,1)S(1)}, bf16[128,1024]{1,0:T(8,128)(2,1)}, u32[]{:S(2)}) copy-start(bf16[128,1024]{1,0:T(8,128)(2,1)} %copy-done.3) | copy-start | bytes 786436
  172.3 36.7 %all-to-all-start.5 = ((bf16[32,8,2048]{2,1,0:T(8,128)(2,1)}), bf16[32,8,2048]{2,1,0:T(8,128)(2,1)S(1)}, u32[]{:S(2)}, u32[]{:S(2)}) async-start(bf16[32,8,2048]{2,1,0:T(8,128)(2,1)} %broadcast_in_dim.11), calls=%async_computation.5 | async-start | bytes 2097152 | tf_op jit(solution)/shard_map/all_to_all | solution.py:62
  176.4 28.9 %copy-start.10 = (bf16[128,2048]{1,0:T(8,128)(2,1)S(1)}, bf16[128,2048]{1,0:T(8,128)(2,1)}, u32[]{:S(2)}) copy-start(bf16[128,2048]{1,0:T(8,128)(2,1)} %copy-done.9) | copy-start | bytes 1572868
  176.4 28.8 %collective-permute-start.7 = (bf16[128,1024]{1,0:T(8,128)(2,1)S(1)}, bf16[128,1024]{1,0:T(8,128)(2,1)S(1)}, u32[]{:S(2)}, u32[]{:S(2)}) collective-permute-start(bf16[128,1024]{1,0:T(8,128)(2,1)S(1)} %copy-done.14), channel_id=1, source_target_pairs={{0,8},{8,0},{1,9},{9,1},{2,10},{10,2},{3,11},{11,3},{4,12},{12,4},... | collective-permute-start | bytes 786440 | tf_op jit(solution)/shard_map/ppermute | solution.py:208
  205.3 1.1 copy-start.8
  205.3 1.6 copy-start.12
  206.4 1.6 copy-start.6
